TPU v7x, 128 devices: a whole 4x4x4 slice. The times are simulated.
128 devices in a mesh: sp: 16 (over z, x), tp: 8 (over y, core).
Axes of the slice: x: 4, y: 4, z: 4, core: 2. Of those that a mesh axis runs over, the one named last changes fastest.
Arguments:
- prompt: bfloat16 [4, 8192, 4096], P(None, 'sp'), may hold values from -6 to 6
- key_weight: bfloat16 [4096, 1024], P(None, 'tp'), may hold values from -0.09375 to 0.09375
- value_weight: bfloat16 [4096, 2048], P(None, 'tp'), may hold values from -0.09375 to 0.09375
- input_gate_weight: bfloat16 [4096, 16], P(None, 'tp'), may hold values from -0.09375 to 0.09375
- forget_gate_weight: bfloat16 [4096, 16], P(None, 'tp'), may hold values from -0.09375 to 0.09375
- forget_bias: float32 [16], P('tp'), may hold values from 3 to 11
- key_taps: bfloat16 [3, 1024], P(None, 'tp'), may hold values from -3 to 3
- extra_decay: float32 [4, 8192, 16], P(None, 'sp', 'tp'), may hold values from -1.5 to 0
- new_query: bfloat16 [4, 16, 64], P(None, 'tp'), may hold values from -6 to 6
- new_key: bfloat16 [4, 16, 64], P(None, 'tp'), may hold values from -6 to 6
- new_value: bfloat16 [4, 16, 128], P(None, 'tp', 'sp'), may hold values from -6 to 6
- new_input_gate: float32 [4, 16], P(None, 'tp'), may hold values from 2 to 7
- new_forget_gate: float32 [4, 16], P(None, 'tp'), may hold values from -2 to 4
- out_weight: bfloat16 [16, 128, 4096], P('tp', 'sp'), may hold values from -0.125 to 0.125
Outputs:
- cache_memory: bfloat16 [4, 16, 64, 128], P(None, 'tp', None, 'sp')
- cache_norm: bfloat16 [4, 16, 64], P(None, 'tp', 'sp')
- cache_peak: float32 [4, 16], P(None, 'tp')
- read_out: bfloat16 [4, 4096], P(None, ('sp', 'tp'))
All inputs are finite; a program needn't handle non-finite values.
Results may differ from a plain program's by a relative error of at most 0.012.
The roundings to bfloat16 on the way count: a program that leaves them out, or rounds other values in their place, can miss the bound.
Values may be sent and summed in bfloat16 or wider, within the bound.
A program may use at most 64 MiB of HBM per device.

v0:
```python
import functools

import jax
import jax.numpy as jnp
from jax import lax
from jax.sharding import Mesh
from jax.sharding import PartitionSpec as P

KEY_DIM = 64
SP = ("sp_0", "sp_1")
SP_TP = ("sp_0", "sp_1", "tp_0", "tp_1")
TP = ("tp_0", "tp_1")


def with_halo(shard, sides, width):
    for axis, dim in sides:
        devices, length = (lax.axis_size(axis), shard.shape[dim])
        up = [(i, (i + 1) % devices) for i in range(devices - 1)]
        down = [(j, i) for i, j in up]
        last = lax.slice_in_dim(shard, length - width, length, axis=dim)
        leading = lax.slice_in_dim(shard, 0, width, axis=dim)
        before = lax.ppermute(last, axis, up)
        after = lax.ppermute(leading, axis, down)
        shard = jnp.concatenate([before, shard, after], axis=dim)
    return shard


def copy_for_each(shard, axis):
    copies = jnp.broadcast_to(shard, (lax.axis_size(axis), *shard.shape))
    return lax.all_to_all(copies, axis, split_axis=0, concat_axis=0, tiled=True)


def joined_by_halves(pieces, combine):
    while len(jax.tree.leaves(pieces)[0]) > 1:
        pieces = jax.vmap(combine)(*(pieces[side::2] for side in (0, 1)))
    return pieces[0]


def prefix(shard, axis, combine, identity):
    devices, here = (lax.axis_size(axis), lax.axis_index(axis))
    passed = jnp.arange(devices) > here

    def kept(part, zero, own):
        part = jnp.where(
            passed.reshape(-1, *(1 for _ in own.shape)), part, jnp.asarray(zero, own.dtype)
        )
        return part[::-1]

    pieces = copy_for_each(shard, axis)
    return joined_by_halves(kept(pieces, identity, shard), combine)


def by_axis(shard, axes):
    return functools.reduce(lax.pmax, axes, shard)


def in_blocks(shard, dim, devices):
    before, after = (shard.shape[:dim], shard.shape[dim + 1 :])
    return jnp.moveaxis(shard.reshape(*before, devices, -1, *after), dim, 0)


def sum_at_owner(shard, axis, dim):
    devices = lax.axis_size(axis)
    parts = lax.all_to_all(in_blocks(shard, dim, devices), axis, 0, 0, tiled=True)
    return jnp.sum(parts, axis=0)


def over_axes(shard, axes):
    for axis in axes:
        shard = lax.psum(shard, axis)
    return shard


def sum_by_axis(shard, axes, dim):
    far, near = axes
    own = sum_at_owner(in_blocks(shard, dim, lax.axis_size(far)), near, dim + 1)
    return jnp.sum(lax.all_to_all(own, far, 0, 0, tiled=True), axis=0)


def widen(rounded):
    return lax.optimization_barrier(rounded).astype(jnp.float32)


def project(seq_rows, key_weight, value_weight, input_gate_weight, forget_gate_weight):
    seq_count, pos_count, width = seq_rows.shape
    flat_rows = seq_rows.reshape(seq_count * pos_count, width)
    key_raw = jnp.dot(flat_rows, key_weight, preferred_element_type=jnp.float32).astype(
        jnp.bfloat16
    )
    values = jnp.dot(flat_rows, value_weight, preferred_element_type=jnp.float32).astype(
        jnp.bfloat16
    )
    gate_weight = jnp.concatenate([input_gate_weight, forget_gate_weight], axis=1)
    gate_pre = jnp.dot(flat_rows, gate_weight, preferred_element_type=jnp.float32).astype(
        jnp.bfloat16
    )
    return (
        key_raw.reshape(seq_count, pos_count, -1),
        values.reshape(seq_count, pos_count, -1),
        gate_pre.reshape(seq_count, pos_count, -1),
    )


def key_conv(padded, key_taps):
    tap_f32 = key_taps.astype(jnp.float32)
    mixed = tap_f32[0] * padded[:, :-2] + tap_f32[1] * padded[:, 1:-1] + tap_f32[2] * padded[:, 2:]
    return (jax.nn.silu(mixed) * KEY_DIM ** (-0.5)).astype(jnp.bfloat16)


def gate_parts(gate_pre, forget_bias, extra):
    head_count = extra.shape[-1]
    gate_f32 = widen(gate_pre)
    input_pre = gate_f32[..., :head_count]
    log_forget = jax.nn.log_sigmoid(gate_f32[..., head_count:] + forget_bias) + extra
    return (input_pre, log_forget)


def suffix_of(log_forget):
    return jnp.sum(log_forget, axis=1, keepdims=True) - jnp.cumsum(log_forget, axis=1)


def add_later(earlier, latter):
    return earlier + latter


def body(
    prompt,
    key_weight,
    value_weight,
    input_gate_weight,
    forget_gate_weight,
    forget_bias,
    key_taps,
    extra_decay,
    new_query,
    new_key,
    new_value,
    new_input_gate,
    new_forget_gate,
    out_weight,
):
    seq_count = prompt.shape[0]
    head_count = extra_decay.shape[-1]
    key_size = new_key.shape[2]
    sp_count = lax.axis_size(SP)
    sp_index = lax.axis_index(SP)
    key_cols = key_size // sp_count
    key_raw, values, gate_pre = project(
        prompt, key_weight, value_weight, input_gate_weight, forget_gate_weight
    )
    input_pre, log_forget = gate_parts(gate_pre, forget_bias, extra_decay)
    padded = with_halo(key_raw, ((SP, 1),), 1)
    key_rows = key_conv(padded, key_taps)
    seg_total = jnp.sum(log_forget, axis=1)
    later_sum = prefix(seg_total, SP, add_later, jnp.zeros_like(seg_total))
    gate_log = input_pre + suffix_of(log_forget) + later_sum[:, None, :]
    peak_log = by_axis(jnp.max(gate_log, axis=1), SP)
    scale = jnp.exp(gate_log - peak_log[:, None, :])
    pos_count = scale.shape[1]
    key_quartet = key_rows.reshape(seq_count, pos_count, head_count, key_size)
    value_four = values.reshape(seq_count, pos_count, head_count, -1)
    weighted_rows = (value_four * scale[..., None]).astype(jnp.bfloat16)
    memory_part = jnp.einsum(
        "slhk,slhv->shkv", key_quartet, weighted_rows, preferred_element_type=jnp.float32
    )
    normer_part = jnp.einsum("slh,slhk->shk", scale, key_quartet.astype(jnp.float32))
    memory_matrix, normer = (sum_at_owner(memory_part, SP, 3), sum_at_owner(normer_part, SP, 2))
    forget_new = jax.nn.log_sigmoid(new_forget_gate)
    new_peak = jnp.maximum(forget_new + peak_log, new_input_gate)
    old_scale = jnp.exp(forget_new + peak_log - new_peak)
    new_scale = jnp.exp(new_input_gate - new_peak)
    key_new = new_key.astype(jnp.float32)
    key_new_slice = lax.dynamic_slice_in_dim(key_new, sp_index * key_cols, key_cols, 2)
    value_new = new_value.astype(jnp.float32)
    memory_next = (
        old_scale[:, :, None, None] * memory_matrix
        + new_scale[:, :, None, None] * key_new[:, :, :, None] * value_new[:, :, None, :]
    )
    normer_next = old_scale[:, :, None] * normer + new_scale[:, :, None] * key_new_slice
    query = new_query.astype(jnp.float32)
    query_slice = lax.dynamic_slice_in_dim(query, sp_index * key_cols, key_cols, 2)
    numer = jnp.sum(query[:, :, :, None] * memory_next, axis=2)
    denom = over_axes(jnp.sum(query_slice * normer_next, axis=-1), SP)
    read = (numer / jnp.maximum(jnp.abs(denom), 1.0)[:, :, None]).astype(jnp.bfloat16)
    partial_value = jnp.einsum("shv,hvd->sd", read, out_weight, preferred_element_type=jnp.float32)
    read_out = sum_by_axis(partial_value, (("sp_0", "sp_1", "tp_0"), "tp_1"), 1).astype(
        jnp.bfloat16
    )
    return (memory_matrix.astype(jnp.bfloat16), normer.astype(jnp.bfloat16), peak_log, read_out)


def solution(mesh):
    torus = Mesh(mesh.devices.reshape(4, 4, 4, 2), ("sp_0", "sp_1", "tp_0", "tp_1"))
    in_specs = (
        P(None, SP, None),
        P(None, TP),
        P(None, TP),
        P(None, TP),
        P(None, TP),
        P(TP),
        P(None, TP),
        P(None, SP, TP),
        P(None, TP, None),
        P(None, TP, None),
        P(None, TP, SP),
        P(None, TP),
        P(None, TP),
        P(TP, SP, None),
    )
    out_specs = (P(None, TP, None, SP), P(None, TP, SP), P(None, TP), P(None, SP_TP))
    return jax.shard_map(body, mesh=torus, in_specs=in_specs, out_specs=out_specs, check_vma=False)
```

profile of v0, /device:TPU:1, one launch (start us, length us, event | category | flops | bytes accessed | tf_op | source)
XLA Modules:
  0.0 141.0 jit_solution(429639210175092399)
XLA Ops:
  0.7 10.7 %convolution_convert_fusion.1 = bf16[2048,128]{1,0:T(8,128)(2,1)S(1)} fusion(bf16[2048,4096]{1,0:T(8,128)(2,1)} %bitcast.56, bf16[4096,128]{1,0:T(8,128)(2,1)} %param.15), kind=kOutput, calls=%fused_computation.3 | convolution fusion | flops 2147745792 | bytes 18350080 | tf_op jit(solution)/shard_map/dot_general | solution.py:87
  11.4 1.3 collective-permute-start.1
  12.7 4.7 %collective-permute-start = (bf16[4,1,128]{2,1,0:T(2,128)(2,1)S(1)}, bf16[4,1,128]{2,1,0:T(2,128)(2,1)S(1)}, u32[]{:S(2)}, u32[]{:S(2)}) collective-permute-start(bf16[4,1,128]{2,1,0:T(2,128)(2,1)S(1)} %get-tuple-element.14), channel_id=1, source_target_pairs={{0,8},{8,16},{16,24},{24,32},{32,40},{40,48},{48,56},{56,64},{64,7... | collective-permute-start | bytes 3080 | tf_op jit(solution)/shard_map/ppermute | solution.py:22
  17.4 10.2 %fusion.1 = bf16[2048,4]{0,1:T(4,128)(2,1)S(1)} fusion(bf16[2048,4096]{1,0:T(8,128)(2,1)} %bitcast.57, bf16[4096,2]{0,1:T(2,128)(2,1)S(1)} %copy-done.2, bf16[4096,2]{0,1:T(2,128)(2,1)S(1)} %copy-done.3), kind=kOutput, calls=%fused_computation.5 | convolution fusion | flops 67182592 | bytes 16826368 | tf_op jit(solution)/shard_map/dot_general | solution.py:94
  28.0 0.6 broadcast_in_dim.15
  28.6 9.5 %all-to-all-start = ((f32[16,4,2]{1,2,0:T(2,128)}), f32[16,4,2]{1,2,0:T(2,128)S(1)}, u32[]{:S(2)}, u32[]{:S(2)}) async-start(f32[16,4,2]{1,2,0:T(2,128)} %broadcast_in_dim.15), calls=%async_computation | async-start | bytes 32768 | tf_op jit(solution)/shard_map/all_to_all | solution.py:30
  38.2 9.4 %fusion = f32[2048,256]{1,0:T(8,128)} fusion(bf16[2048,4096]{1,0:T(8,128)(2,1)} %bitcast.58, bf16[4096,256]{1,0:T(8,128)(2,1)S(1)} %copy-done), kind=kOutput, calls=%fused_computation.2 | convolution fusion | flops 4296015872 | bytes 20971520 | tf_op jit(solution)/shard_map/dot_general | solution.py:90
  47.6 3.4 %reshape.78 = f32[4,512,2,128]{3,2,1,0:T(2,128)} reshape(f32[2048,256]{1,0:T(8,128)} %fusion) | data formatting | bytes 4194304 | tf_op jit(solution)/shard_map/convert_element_type | solution.py:162
  51.0 2.4 %reduce-window.6 = f32[4,2,4,128]{3,2,1,0:T(4,128)S(1)} reduce-window(f32[4,2,4,128]{3,2,1,0:T(4,128)S(1)} %reshape.72, f32[]{:T(128)} %constant.15.clone.1), window={size=1x1x1x128 pad=0_0x0_0x0_0x127_0}, to_apply=%region_1.2 | reduce-window | flops 520192 | bytes 32772 | tf_op jit(solution)/shard_map/reduce-window
  53.6 0.7 reduce-window.9
  55.1 8.5 %pmax.14 = f32[4,2]{1,0:T(4,128)S(1)} all-reduce(f32[4,2]{1,0:T(4,128)S(1)} %fusion.21), channel_id=1, replica_groups=mesh['sp_0'=4,'sp_1'=4,'tp_0'=4,'tp_1'=2] {'sp_0'}, use_global_device_ids=true, to_apply=%region_4.5 | all-reduce | flops 8 | bytes 64 | tf_op jit(solution)/shard_map/pmax | solution.py:54
  63.6 8.6 %pmax.15 = f32[4,2]{1,0:T(4,128)S(1)} all-reduce(f32[4,2]{1,0:T(4,128)S(1)} %pmax.14), channel_id=1, replica_groups=mesh['sp_0'=4,'sp_1'=4,'tp_0'=4,'tp_1'=2] {'sp_1'}, use_global_device_ids=true, to_apply=%region_5.6 | all-reduce | flops 8 | bytes 64 | tf_op jit(solution)/shard_map/pmax | solution.py:54
  72.3 0.6 multiply_convert_fusion
  73.6 0.7 copy.63
  74.2 3.5 %all-to-all-start.2 = ((f32[16,4,2,4]{3,2,1,0:T(2,128)}), f32[16,4,2,4]{3,2,1,0:T(2,128)S(1)}, u32[]{:S(2)}, u32[]{:S(2)}) async-start(f32[16,4,2,4]{3,2,1,0:T(2,128)} %copy.63), calls=%async_computation.2 | async-start | bytes 131072 | tf_op jit(solution)/shard_map/all_to_all | solution.py:64
  77.7 2.8 %convolution_bitcast_fusion.1 = f32[16,4,2,64,8]{3,4,0,2,1:T(8,128)S(1)} fusion(bf16[4,512,2,64]{1,3,2,0:T(8,128)(2,1)S(1)} %bitcast.61, f32[4,512,2,128]{3,2,1,0:T(2,128)} %reshape.78, f32[4,512,2]{1,2,0:T(2,128)S(1)} %subtract_exponential_fusion), kind=kOutput, calls=%fused_computation.8 | convolution fusion | flops 68157440 | bytes 2899968 | tf_op jit(solution)/shard_map/slhk,slhv->shkv/dot_general | solution.py:163
  80.6 1.0 reshape.83
  81.6 2.5 %all-to-all-done.2 = f32[16,4,2,4]{3,2,1,0:T(2,128)S(1)} async-done(((f32[16,4,2,4]{3,2,1,0:T(2,128)}), f32[16,4,2,4]{3,2,1,0:T(2,128)S(1)}, u32[]{:S(2)}, u32[]{:S(2)}) %all-to-all-start.2) | async-done | bytes 2080 | tf_op jit(solution)/shard_map/all_to_all | solution.py:64
  84.2 4.1 %all-to-all-start.1 = ((f32[16,1,4096]{2,1,0:T(1,128)}), f32[16,1,4096]{2,1,0:T(1,128)S(1)}, u32[]{:S(2)}, u32[]{:S(2)}) async-start(f32[16,1,4096]{2,1,0:T(1,128)} %reshape.83), calls=%async_computation.1 | async-start | bytes 524288 | tf_op jit(solution)/shard_map/all_to_all | solution.py:64
  88.3 0.6 multiply_reduce_fusion.1
  88.9 8.5 %psum.14 = f32[4,2]{1,0:T(4,128)S(1)} all-reduce(f32[4,2]{1,0:T(4,128)S(1)} %get-tuple-element.22), channel_id=1, replica_groups=mesh['sp_0'=4,'sp_1'=4,'tp_0'=4,'tp_1'=2] {'sp_0'}, use_global_device_ids=true, to_apply=%region_10.11 | all-reduce | flops 8 | bytes 64 | tf_op jit(solution)/shard_map/psum | solution.py:70
  97.5 8.4 %psum.15 = f32[4,2]{1,0:T(4,128)S(1)} all-reduce(f32[4,2]{1,0:T(4,128)S(1)} %psum.14), channel_id=1, replica_groups=mesh['sp_0'=4,'sp_1'=4,'tp_0'=4,'tp_1'=2] {'sp_1'}, use_global_device_ids=true, to_apply=%region_11.12 | all-reduce | flops 8 | bytes 64 | tf_op jit(solution)/shard_map/psum | solution.py:70
  106.4 1.3 reduce.2
  107.9 0.7 multiply_reduce_fusion
  109.3 14.2 %all_to_all.25 = f32[2,1,8192]{2,1,0:T(1,128)S(1)} all-to-all(f32[2,1,8192]{2,1,0:T(1,128)S(1)} %reshape.85), channel_id=1, replica_groups=mesh['sp_0'=4,'sp_1'=4,'tp_0'=4,'tp_1'=2] {'tp_1'}, dimensions={0} | all-to-all | bytes 131072 | tf_op jit(solution)/shard_map/all_to_all | solution.py:64
  123.5 0.8 reduce.3
  124.6 0.7 reshape.87
  125.3 5.8 %all-to-all-start.4 = ((f32[64,1,128]{2,1,0:T(1,128)}), f32[64,1,128]{2,1,0:T(1,128)S(1)}, u32[]{:S(2)}, u32[]{:S(2)}) async-start(f32[64,1,128]{2,1,0:T(1,128)} %reshape.87), calls=%async_computation.4 | async-start | bytes 65536 | tf_op jit(solution)/shard_map/all_to_all | solution.py:77
  131.1 0.6 copy.72
  131.8 7.8 %all-to-all-done.4 = f32[64,1,128]{2,1,0:T(1,128)S(1)} async-done(((f32[64,1,128]{2,1,0:T(1,128)}), f32[64,1,128]{2,1,0:T(1,128)S(1)}, u32[]{:S(2)}, u32[]{:S(2)}) %all-to-all-start.4) | async-done | bytes 32800 | tf_op jit(solution)/shard_map/all_to_all | solution.py:77
  139.5 0.7 reduce.4
  140.4 0.6 reduce_sum.73
  (75 shorter events, 3.9 us)
Async XLA Ops:
  0.6 37.6 %copy-start = (bf16[4096,256]{1,0:T(8,128)(2,1)S(1)}, bf16[4096,256]{1,0:T(8,128)(2,1)}, u32[]{:S(2)}) copy-start(bf16[4096,256]{1,0:T(8,128)(2,1)} %param.16) | copy-start | bytes 6291460
  0.6 16.8 %copy-start.2 = (bf16[4096,2]{0,1:T(2,128)(2,1)S(1)}, bf16[4096,2]{0,1:T(2,128)(2,1)}, u32[]{:S(2)}) copy-start(bf16[4096,2]{0,1:T(2,128)(2,1)} %param.18) | copy-start | bytes 49156
  0.7 16.8 %copy-start.3 = (bf16[4096,2]{0,1:T(2,128)(2,1)S(1)}, bf16[4096,2]{0,1:T(2,128)(2,1)}, u32[]{:S(2)}) copy-start(bf16[4096,2]{0,1:T(2,128)(2,1)} %param.17) | copy-start | bytes 49156
  11.4 61.0 %collective-permute-start.1 = (bf16[4,1,128]{2,1,0:T(2,128)(2,1)S(1)}, bf16[4,1,128]{2,1,0:T(2,128)(2,1)S(1)}, u32[]{:S(2)}, u32[]{:S(2)}) collective-permute-start(bf16[4,1,128]{2,1,0:T(2,128)(2,1)S(1)} %get-tuple-element.15), channel_id=1, source_target_pairs={{8,0},{16,8},{24,16},{32,24},{40,32},{48,40},{56,48},{64,56},{72,6... | collective-permute-start | bytes 3080 | tf_op jit(solution)/shard_map/ppermute | solution.py:23
  12.7 15.0 %copy-start.4 = (f32[4,512,2]{1,2,0:T(2,128)S(1)}, f32[4,512,2]{1,2,0:T(2,128)}, u32[]{:S(2)}) copy-start(f32[4,512,2]{1,2,0:T(2,128)} %param.21) | copy-start | bytes 49156
  12.7 15.0 %copy-start.11 = (f32[2]{0:T(128)S(1)}, f32[2]{0:T(128)}, u32[]{:S(2)}) copy-start(f32[2]{0:T(128)} %param.19) | copy-start | bytes 28
  12.7 25.5 %copy-start.8 = (bf16[3,128]{1,0:T(4,128)(2,1)S(1)}, bf16[3,128]{1,0:T(4,128)(2,1)}, u32[]{:S(2)}) copy-start(bf16[3,128]{1,0:T(4,128)(2,1)} %param.20) | copy-start | bytes 2308
  12.7 59.6 %collective-permute-start = (bf16[4,1,128]{2,1,0:T(2,128)(2,1)S(1)}, bf16[4,1,128]{2,1,0:T(2,128)(2,1)S(1)}, u32[]{:S(2)}, u32[]{:S(2)}) collective-permute-start(bf16[4,1,128]{2,1,0:T(2,128)(2,1)S(1)} %get-tuple-element.14), channel_id=1, source_target_pairs={{0,8},{8,16},{16,24},{24,32},{32,40},{40,48},{48,56},{56,64},{64,7... | collective-permute-start | bytes 3080 | tf_op jit(solution)/shard_map/ppermute | solution.py:22
  28.6 26.1 %all-to-all-start = ((f32[16,4,2]{1,2,0:T(2,128)}), f32[16,4,2]{1,2,0:T(2,128)S(1)}, u32[]{:S(2)}, u32[]{:S(2)}) async-start(f32[16,4,2]{1,2,0:T(2,128)} %broadcast_in_dim.15), calls=%async_computation | async-start | bytes 32768 | tf_op jit(solution)/shard_map/all_to_all | solution.py:30
  47.6 6.8 %copy-start.6 = (bf16[4,2,8]{2,1,0:T(2,128)(2,1)S(1)}, bf16[4,2,8]{2,1,0:T(2,128)(2,1)}, u32[]{:S(2)}) copy-start(bf16[4,2,8]{2,1,0:T(2,128)(2,1)} %param.24) | copy-start | bytes 388
  47.6 6.8 %copy-start.9 = (f32[4,2]{0,1:T(2,128)S(1)}, f32[4,2]{0,1:T(2,128)}, u32[]{:S(2)}) copy-start(f32[4,2]{0,1:T(2,128)} %param.25) | copy-start | bytes 100
  47.6 6.9 %copy-start.10 = (f32[4,2]{0,1:T(2,128)S(1)}, f32[4,2]{0,1:T(2,128)}, u32[]{:S(2)}) copy-start(f32[4,2]{0,1:T(2,128)} %param.26) | copy-start | bytes 100
  47.6 7.0 %copy-start.7 = (bf16[4,2,64]{2,1,0:T(2,128)(2,1)S(1)}, bf16[4,2,64]{2,1,0:T(2,128)(2,1)}, u32[]{:S(2)}) copy-start(bf16[4,2,64]{2,1,0:T(2,128)(2,1)} %param.22) | copy-start | bytes 3076
  47.6 7.0 %copy-start.5 = (bf16[4,2,64]{2,1,0:T(2,128)(2,1)S(1)}, bf16[4,2,64]{2,1,0:T(2,128)(2,1)}, u32[]{:S(2)}) copy-start(bf16[4,2,64]{2,1,0:T(2,128)(2,1)} %param.23) | copy-start | bytes 3076
  74.2 10.0 %all-to-all-start.2 = ((f32[16,4,2,4]{3,2,1,0:T(2,128)}), f32[16,4,2,4]{3,2,1,0:T(2,128)S(1)}, u32[]{:S(2)}, u32[]{:S(2)}) async-start(f32[16,4,2,4]{3,2,1,0:T(2,128)} %copy.63), calls=%async_computation.2 | async-start | bytes 131072 | tf_op jit(solution)/shard_map/all_to_all | solution.py:64
  80.5 28.1 %copy-start.1 = (bf16[2,8,4096]{2,1,0:T(8,128)(2,1)S(1)}, bf16[2,8,4096]{2,1,0:T(8,128)(2,1)}, u32[]{:S(2)}) copy-start(bf16[2,8,4096]{2,1,0:T(8,128)(2,1)} %param.27) | copy-start | bytes 393220
  84.2 21.7 %all-to-all-start.1 = ((f32[16,1,4096]{2,1,0:T(1,128)}), f32[16,1,4096]{2,1,0:T(1,128)S(1)}, u32[]{:S(2)}, u32[]{:S(2)}) async-start(f32[16,1,4096]{2,1,0:T(1,128)} %reshape.83), calls=%async_computation.1 | async-start | bytes 524288 | tf_op jit(solution)/shard_map/all_to_all | solution.py:64
  125.3 14.2 %all-to-all-start.4 = ((f32[64,1,128]{2,1,0:T(1,128)}), f32[64,1,128]{2,1,0:T(1,128)S(1)}, u32[]{:S(2)}, u32[]{:S(2)}) async-start(f32[64,1,128]{2,1,0:T(1,128)} %reshape.87), calls=%async_computation.4 | async-start | bytes 65536 | tf_op jit(solution)/shard_map/all_to_all | solution.py:77
where the time goes:
time: 142 us; the launch traced here: 141 us
  blocking collectives  48.2 us (34%)
  matrix products  33.6 us (24%)
  starting transfers between devices  28.9 us (20%)
  waiting for transfers between devices  10.3 us (7%)
  local copies, waits for them, and re-layouts  9.54 us (7%)
  other arithmetic  9.47 us (7%)
    pmax x2, blocking collectives, by_axis(): return functools.reduce(lax.pmax, axes, shard)  17.1 us
    psum x2, blocking collectives, over_axes(): shard = lax.psum(shard, axis)  16.9 us
    all_to_all x1, blocking collectives, sum_at_owner(): lax.all_to_all(in_blocks(shard, dim, devices), axis, 0, 0, tiled=True)  14.2 us
    dot_general x1, matrix products, project(): jnp.dot(flat_rows, key_weight, preferred_element_type=jnp.float32)  10.7 us
    dot_general x1, matrix products, project(): jnp.dot(flat_rows, gate_weight, preferred_element_type=jnp.float32)  10.2 us
    all_to_all x1, starting transfers between devices, copy_for_each(): return lax.all_to_all(copies, axis, split_axis=0, concat_axis=0, tiled=True)  9.52 us
    dot_general x1, matrix products, project(): jnp.dot(flat_rows, value_weight, preferred_element_type=jnp.float32)  9.43 us
    all_to_all x1, waiting for transfers between devices, sum_by_axis(): return jnp.sum(lax.all_to_all(own, far, 0, 0, tiled=True), axis=0)  7.78 us
  transfers between devices with their start and end apart: 6, of which 2 were waited for; matrix products, arithmetic and copies ran while one was open for 24% of the time, Pallas kernels for 0%

commit v1 on v0

v1 whole, which is shorter than its diff:
```python
import jax
import jax.numpy as jnp
from jax import lax
from jax.experimental import pallas as pl
from jax.experimental.pallas import tpu as pltpu
from jax.sharding import PartitionSpec as P

MESH_ID = pl.DeviceIdType.MESH
F32 = jnp.float32
BF16 = jnp.bfloat16
NT = (((1,), (1,)), ((), ()))
KEY0 = 16
VAL0 = 144
CHUNKS = 4


def log_sigmoid(x):
    return jnp.minimum(x, 0.0) - jnp.log1p(jnp.exp(-jnp.abs(x)))


def three_parts(x):
    high = x.astype(BF16)
    rest = x - high.astype(F32)
    middle = rest.astype(BF16)
    low = (rest - middle.astype(F32)).astype(BF16)
    return high, middle, low


def kernel(
    prompt, key_w, value_w, in_w, fg_w, fg_bias, taps, extra, query, new_key, new_value,
    new_in, new_fg, out_w,
    mem_out, norm_out, peak_out, read_out,
    p_buf, wk_buf, wv_buf, wt_buf, hp_buf, r_buf, par_buf, mem_buf, e_buf,
    h_send, h_recv, e_recv, m_recv, ow_recv, part_buf, part_recv,
    w_sem, p_sem, hp_sem, ow_local, h_ssem, h_rsem, e_ssem, e_rsem, m_ssem, m_rsem,
    ow_ssem, ow_rsem, o_ssem, o_rsem,
):
    seqs, length, width = p_buf.shape
    sp_n, tp_n = lax.axis_size("sp"), lax.axis_size("tp")
    sp, tp = lax.axis_index("sp"), lax.axis_index("tp")
    step = width // CHUNKS

    barrier = pltpu.get_barrier_semaphore()

    def sp_peer(d):
        return lax.rem(sp + d, sp_n)

    def tp_peer(d):
        return lax.rem(tp + d, tp_n)

    @pl.loop(1, sp_n)
    def _(d):
        pl.semaphore_signal(barrier, inc=1, device_id=(sp_peer(d), tp), device_id_type=MESH_ID)

    @pl.loop(1, tp_n)
    def _(d):
        pl.semaphore_signal(barrier, inc=1, device_id=(sp, tp_peer(d)), device_id_type=MESH_ID)

    hp_copies = []
    for s in range(seqs):
        for side, row in ((0, 0), (1, length - 8)):
            g = 2 * s + side
            hp_copies.append(
                pltpu.make_async_copy(
                    prompt.at[s, pl.ds(row, 8), :], hp_buf.at[pl.ds(8 * g, 8), :], hp_sem.at[g]
                )
            )
    w_copies, p_copies = [], []
    for c in range(CHUNKS):
        rows = pl.ds(c * step, step)
        w_copies.append(
            (
                pltpu.make_async_copy(key_w.at[rows, :], wk_buf.at[rows, :], w_sem.at[0, c]),
                pltpu.make_async_copy(value_w.at[rows, :], wv_buf.at[rows, :], w_sem.at[1, c]),
            )
        )
        p_copies.append(
            pltpu.make_async_copy(prompt.at[0, :, rows], p_buf.at[0, :, rows], p_sem.at[0, c])
        )
    for c in range(CHUNKS):
        for copy in w_copies[c]:
            copy.start()
        p_copies[c].start()
        if c == 0:
            for copy in hp_copies:
                copy.start()
    s_copies = [None]
    for s in range(1, seqs):
        group = []
        for c in range(CHUNKS):
            rows = pl.ds(c * (length // CHUNKS), length // CHUNKS)
            group.append(
                pltpu.make_async_copy(prompt.at[s, rows, :], p_buf.at[s, rows, :], p_sem.at[s, c])
            )
        for copy in group:
            copy.start()
        s_copies.append(group)

    lane = lax.broadcasted_iota(jnp.int32, (1, 128), 1)
    first_head = lane < 64

    def halves(left, right):
        return jnp.where(first_head, left, right)

    for s in range(seqs):
        rows = pl.ds(s, 1)
        par_buf[0, rows, :] = jnp.concatenate(
            [query[s, 0:1, :].astype(F32), query[s, 1:2, :].astype(F32)], axis=1
        )
        par_buf[1, rows, :] = jnp.concatenate(
            [new_key[s, 0:1, :].astype(F32), new_key[s, 1:2, :].astype(F32)], axis=1
        )
        par_buf[2, rows, :] = halves(new_in[0:1, s : s + 1], new_in[1:2, s : s + 1])
        par_buf[3, rows, :] = halves(new_fg[0:1, s : s + 1], new_fg[1:2, s : s + 1])
    tap_cols = jnp.transpose(
        jnp.concatenate([taps[...].astype(F32), jnp.zeros((5, 128), F32)], axis=0)
    )
    q_cols = jnp.transpose(
        jnp.concatenate([par_buf[0, 0:4, :], jnp.zeros((4, 128), F32)], axis=0)
    )
    gate_rows = jnp.concatenate(
        [
            in_w[...].astype(F32), jnp.zeros((6, width), F32),
            fg_w[...].astype(F32), jnp.zeros((6, width), F32),
        ],
        axis=0,
    )
    wt_buf[0:KEY0, :] = gate_rows.astype(BF16)

    for c in range(CHUNKS):
        cols = pl.ds(c * step, step)
        for copy in w_copies[c]:
            copy.wait()
        wt_buf[KEY0:VAL0, cols] = jnp.transpose(wk_buf[cols, :])
        wt_buf[VAL0:, cols] = jnp.transpose(wv_buf[cols, :])
        p_copies[c].wait()
        part = lax.dot_general(
            wt_buf[:, cols], p_buf[0, :, cols], NT, preferred_element_type=F32
        )
        if c == 0:
            r_buf[0] = part
        else:
            r_buf[0] = r_buf[0] + part

    for copy in hp_copies:
        copy.wait()
    edge = jnp.dot(hp_buf[...], wk_buf[...], preferred_element_type=F32).astype(BF16).astype(F32)
    zero4 = jnp.zeros((4, 128), F32)
    h_send[0] = jnp.concatenate(
        [edge[16 * s + 15 : 16 * s + 16] for s in range(seqs)] + [zero4], axis=0
    )
    h_send[1] = jnp.concatenate(
        [edge[16 * s : 16 * s + 1] for s in range(seqs)] + [zero4], axis=0
    )

    pl.semaphore_wait(barrier, sp_n - 1 + tp_n - 1)

    cols_of = out_w.shape[2] // sp_n

    def ow_slot(ref):
        return ref.at[sp // 8, :, lax.rem(sp, 8)]

    def ow_cols(j):
        return out_w.at[:, :, pl.ds(pl.multiple_of(j * cols_of, cols_of), cols_of)]

    own_ow = pltpu.make_async_copy(ow_cols(sp), ow_slot(ow_recv), ow_local)
    own_ow.start()

    halo_copies = []
    for side, d in ((0, 1), (1, sp_n - 1)):
        copy = pltpu.make_async_remote_copy(
            src_ref=h_send.at[side],
            dst_ref=h_recv.at[side],
            send_sem=h_ssem.at[side],
            recv_sem=h_rsem.at[side],
            device_id=(sp_peer(d), tp),
            device_id_type=MESH_ID,
        )
        copy.start()
        halo_copies.append(copy)

    @pl.loop(1, sp_n)
    def _(d):
        j = sp_peer(d)
        pltpu.make_async_remote_copy(
            src_ref=ow_cols(j),
            dst_ref=ow_slot(ow_recv),
            send_sem=ow_ssem,
            recv_sem=ow_rsem,
            device_id=(j, tp),
            device_id_type=MESH_ID,
        ).start()

    def edges():
        for copy in halo_copies:
            copy.wait_recv()
        before = jnp.where(sp == 0, 0.0, jnp.transpose(h_recv[0]))
        after = jnp.where(sp == sp_n - 1, 0.0, jnp.transpose(h_recv[1]))
        return before, after

    pos = lax.broadcasted_iota(jnp.int32, (1, length), 1)
    my_rows = pl.multiple_of(8 * sp, 8)

    def slot_rows(s):
        return pl.ds(pl.multiple_of((s * sp_n + sp) * 8, 8), 8)

    def finish(s, before, after):
        buf = s % 2
        in_pre = r_buf[buf, 0:2, :].astype(BF16).astype(F32)
        fg_pre = r_buf[buf, 8:10, :].astype(BF16).astype(F32)
        log_f = log_sigmoid(fg_pre + fg_bias[...]) + extra[s]
        later = jnp.where(pos < length - 1, pltpu.roll(log_f, length - 1, 1), 0.0)
        shift = 1
        while shift < length:
            later = later + jnp.where(
                pos < length - shift, pltpu.roll(later, length - shift, 1), 0.0
            )
            shift *= 2
        total = later[:, 0:1] + log_f[:, 0:1]
        gate = in_pre + later
        top = jnp.max(gate, axis=1, keepdims=True)
        scale = jnp.exp(gate - top)

        key = r_buf[buf, KEY0:VAL0, :].astype(BF16).astype(F32)
        earlier = jnp.where(pos == 0, before[:, s : s + 1], pltpu.roll(key, 1, 1))
        coming = jnp.where(pos == length - 1, after[:, s : s + 1], pltpu.roll(key, length - 1, 1))
        mixed = tap_cols[:, 0:1] * earlier + tap_cols[:, 1:2] * key + tap_cols[:, 2:3] * coming
        key_rows = (mixed * jax.nn.sigmoid(mixed) * 0.125).astype(BF16)
        prod = key_rows.astype(F32) * q_cols[:, s : s + 1]
        along = jnp.concatenate(
            [
                jnp.sum(prod[0:64], axis=0, keepdims=True),
                jnp.sum(prod[64:128], axis=0, keepdims=True),
            ],
            axis=0,
        )
        value = r_buf[buf, VAL0:, :].astype(BF16).astype(F32)
        weighted = jnp.concatenate(
            [
                (value[0:128] * scale[0:1]).astype(BF16),
                (value[128:256] * scale[1:2]).astype(BF16),
            ],
            axis=0,
        )

        def rows_of(x):
            parts = [part.astype(F32) for part in three_parts(x)]
            return jnp.concatenate(parts + [jnp.zeros((10, length), F32)], axis=0).astype(BF16)

        norm_parts = lax.dot_general(rows_of(scale), key_rows, NT, preferred_element_type=F32)
        num_parts = lax.dot_general(rows_of(along), weighted, NT, preferred_element_type=F32)
        outer = lax.dot_general(weighted, key_rows, NT, preferred_element_type=F32)
        mem_buf[pl.ds(128 * s, 128), :] = halves(outer[0:128], outer[128:256])

        def joined(x, h):
            return x[h : h + 1] + x[2 + h : 3 + h] + x[4 + h : 5 + h]

        norm = halves(joined(norm_parts, 0), joined(norm_parts, 1))
        num0 = joined(num_parts, 0)[:, 0:128]
        num1 = joined(num_parts, 1)[:, 128:256]
        num_a = halves(num0, pltpu.roll(num1, 64, 1))
        num_b = halves(pltpu.roll(num0, 64, 1), num1)

        fresh = new_value[s].astype(F32)
        spread = jnp.concatenate([fresh, jnp.zeros((2, 120), F32)], axis=1)
        left = pltpu.roll(spread, 8 * lax.rem(sp, 8), 1)
        fresh_row = halves(left[0:1], pltpu.roll(left[1:2], 64, 1))
        fresh_a = jnp.where(sp < 8, fresh_row, 0.0)
        fresh_b = jnp.where(sp < 8, 0.0, fresh_row)
        tile = jnp.concatenate(
            [
                norm,
                halves(total[0:1], total[1:2]),
                halves(top[0:1], top[1:2]),
                num_a,
                num_b,
                fresh_a,
                fresh_b,
                jnp.zeros((1, 128), F32),
            ],
            axis=0,
        )
        e_buf[pl.ds(8 * s, 8), :] = tile
        e_recv[slot_rows(s), :] = tile
        m_recv[slot_rows(s), :] = mem_buf[pl.ds(128 * s + my_rows, 8), :]

        @pl.loop(1, sp_n)
        def _(d):
            pltpu.make_async_remote_copy(
                src_ref=e_buf.at[pl.ds(8 * s, 8), :],
                dst_ref=e_recv.at[slot_rows(s), :],
                send_sem=e_ssem.at[s],
                recv_sem=e_rsem.at[s],
                device_id=(sp_peer(d), tp),
                device_id_type=MESH_ID,
            ).start()

        @pl.loop(1, sp_n)
        def _(d):
            j = sp_peer(d)
            pltpu.make_async_remote_copy(
                src_ref=mem_buf.at[pl.ds(pl.multiple_of(128 * s + 8 * j, 8), 8), :],
                dst_ref=m_recv.at[slot_rows(s), :],
                send_sem=m_ssem.at[s],
                recv_sem=m_rsem.at[s],
                device_id=(j, tp),
                device_id_type=MESH_ID,
            ).start()

    before = after = None
    for s in range(1, seqs):
        for copy in s_copies[s]:
            copy.wait()
        if s == 1:
            before, after = edges()
        r_buf[s % 2] = lax.dot_general(wt_buf[...], p_buf[s], NT, preferred_element_type=F32)
        finish(s - 1, before, after)
    finish(seqs - 1, before, after)

    def take(ref, sem, count):
        view = ref.at[pl.ds(0, count), :]
        pltpu.make_async_copy(view, view, sem).wait()

    own_ow.wait()

    row16 = lax.broadcasted_iota(jnp.int32, (sp_n, 128), 0)
    reads, factors = [], []
    for s in range(seqs):
        take(e_recv, e_rsem.at[s], 8 * (sp_n - 1))
    for s in range(seqs):

        def rows_at(k):
            return e_recv[pl.ds(s * sp_n * 8 + k, sp_n, stride=8), :]

        later = jnp.where(row16 < sp_n - 1, pltpu.roll(rows_at(1), sp_n - 1, 0), 0.0)
        shift = 1
        while shift < sp_n:
            later = later + jnp.where(
                row16 < sp_n - shift, pltpu.roll(later, sp_n - shift, 0), 0.0
            )
            shift *= 2
        gate = rows_at(2) + later
        peak = jnp.max(gate, axis=0, keepdims=True)
        factor = jnp.exp(gate - peak)
        factors.append(factor)

        def summed(k):
            return jnp.sum(factor * rows_at(k), axis=0, keepdims=True)

        norm, num_a, num_b = summed(0), summed(3), summed(4)
        fresh_a = jnp.sum(rows_at(5), axis=0, keepdims=True)
        fresh_b = jnp.sum(rows_at(6), axis=0, keepdims=True)
        q, k = par_buf[0, s : s + 1, :], par_buf[1, s : s + 1, :]
        gate_in, gate_fg = par_buf[2, s : s + 1, :], par_buf[3, s : s + 1, :]
        kept = log_sigmoid(gate_fg) + peak
        new_peak = jnp.maximum(kept, gate_in)
        old_scale = jnp.exp(kept - new_peak)
        new_scale = jnp.exp(gate_in - new_peak)

        def by_head(x):
            left = jnp.sum(jnp.where(first_head, x, 0.0), axis=1, keepdims=True)
            right = jnp.sum(jnp.where(first_head, 0.0, x), axis=1, keepdims=True)
            return halves(left, right)

        denom = jnp.maximum(jnp.abs(by_head(q * (old_scale * norm + new_scale * k))), 1.0)
        fresh_scale = new_scale * by_head(q * k)
        read_a = (old_scale * num_a + fresh_scale * fresh_a) / denom
        read_b = (old_scale * num_b + fresh_scale * fresh_b) / denom
        reads.append(jnp.concatenate([read_a, read_b], axis=1))
        mine = pltpu.roll(norm, lax.rem(128 - 4 * sp, 128), 1).astype(BF16)
        norm_out[s, 0:1, :] = mine[:, 0:4]
        norm_out[s, 1:2, :] = mine[:, 64:68]
        peak_out[0:1, s : s + 1] = peak[:, 0:1]
        peak_out[1:2, s : s + 1] = peak[:, 64:65]

    ow_words = pltpu.make_async_copy(
        out_w.at[:, :, pl.ds(0, cols_of * (sp_n - 1))],
        out_w.at[:, :, pl.ds(0, cols_of * (sp_n - 1))],
        ow_rsem,
    )
    ow_words.wait()
    read = jnp.concatenate(reads + [jnp.zeros((12, 256), F32)], axis=0).astype(BF16)
    weight = ow_recv[...].reshape(256, cols_of)
    part = jnp.dot(read, weight, preferred_element_type=F32)[0:8]
    part_buf[...] = part
    part_recv[tp] = part

    @pl.loop(1, tp_n)
    def _(d):
        pltpu.make_async_remote_copy(
            src_ref=part_buf,
            dst_ref=part_recv.at[tp],
            send_sem=o_ssem,
            recv_sem=o_rsem,
            device_id=(sp, tp_peer(d)),
            device_id_type=MESH_ID,
        ).start()

    for s in range(seqs):
        take(m_recv, m_rsem.at[s], 8 * (sp_n - 1))
    for s in range(seqs):
        memory = jnp.zeros((8, 128), F32)
        for i in range(sp_n):
            base = (s * sp_n + i) * 8
            memory = memory + factors[s][i : i + 1] * m_recv[base : base + 8, :]
        mem_out[s, 0] = memory[:, 0:64].astype(BF16)
        mem_out[s, 1] = memory[:, 64:128].astype(BF16)

    view = part_recv.at[pl.ds(0, tp_n - 1)]
    pltpu.make_async_copy(view, view, o_rsem).wait()
    whole = part_recv[0]
    for i in range(1, tp_n):
        whole = whole + part_recv[i]
    turned = pltpu.roll(whole, lax.rem(cols_of - 32 * tp, cols_of), 1)
    read_out[...] = turned[0:4, 0:32].astype(BF16)

    for copy in halo_copies:
        copy.wait_send()
    pltpu.make_async_copy(
        out_w.at[:, :, pl.ds(0, cols_of * (sp_n - 1))],
        out_w.at[:, :, pl.ds(0, cols_of * (sp_n - 1))],
        ow_ssem,
    ).wait()
    for s in range(seqs):
        take(e_recv, e_ssem.at[s], 8 * (sp_n - 1))
        take(m_recv, m_ssem.at[s], 8 * (sp_n - 1))
    pltpu.make_async_copy(view, view, o_ssem).wait()


def body(
    prompt, key_weight, value_weight, input_gate_weight, forget_gate_weight, forget_bias,
    key_taps, extra_decay, new_query, new_key, new_value, new_input_gate, new_forget_gate,
    out_weight,
):
    seqs, length, width = prompt.shape
    sp_n = lax.axis_size("sp")
    tp_n = lax.axis_size("tp")
    cols_of = out_weight.shape[2] // sp_n
    any_spec = pl.BlockSpec(memory_space=pl.ANY)
    vmem = pl.BlockSpec(memory_space=pltpu.VMEM)
    dma = pltpu.SemaphoreType.DMA
    memory, norm, peak, read = pl.pallas_call(
        kernel,
        out_shape=(
            jax.ShapeDtypeStruct((seqs, 2, 8, 64), BF16),
            jax.ShapeDtypeStruct((seqs, 2, 4), BF16),
            jax.ShapeDtypeStruct((2, seqs), F32),
            jax.ShapeDtypeStruct((seqs, 32), BF16),
        ),
        in_specs=[any_spec] * 3 + [vmem] * 10 + [any_spec],
        out_specs=(vmem,) * 4,
        scratch_shapes=[
            pltpu.VMEM((seqs, length, width), BF16),
            pltpu.VMEM((width, 128), BF16),
            pltpu.VMEM((width, 256), BF16),
            pltpu.VMEM((400, width), BF16),
            pltpu.VMEM((64, width), BF16),
            pltpu.VMEM((2, 400, length), F32),
            pltpu.VMEM((4, 8, 128), F32),
            pltpu.VMEM((seqs * 128, 128), F32),
            pltpu.VMEM((seqs * 8, 128), F32),
            pltpu.VMEM((2, 8, 128), F32),
            pltpu.VMEM((2, 8, 128), F32),
            pltpu.VMEM((seqs * sp_n * 8, 128), F32),
            pltpu.VMEM((seqs * sp_n * 8, 128), F32),
            pltpu.VMEM((2, 2, 8, 8, cols_of), BF16),
            pltpu.VMEM((8, cols_of), F32),
            pltpu.VMEM((tp_n, 8, cols_of), F32),
            dma((2, CHUNKS)),
            dma((seqs, CHUNKS)),
            dma((2 * seqs,)),
            dma,
            dma((2,)),
            dma((2,)),
            dma((seqs,)),
            dma((seqs,)),
            dma((seqs,)),
            dma((seqs,)),
            dma,
            dma,
            dma,
            dma,
        ],
        compiler_params=pltpu.CompilerParams(
            collective_id=0, has_side_effects=True, vmem_limit_bytes=60 * 1024 * 1024
        ),
        name="prompt_state",
    )(
        prompt,
        key_weight,
        value_weight,
        input_gate_weight.T,
        forget_gate_weight.T,
        forget_bias.reshape(2, 1),
        key_taps,
        jnp.transpose(extra_decay, (0, 2, 1)),
        new_query,
        new_key,
        new_value,
        new_input_gate.T,
        new_forget_gate.T,
        out_weight,
    )
    return jnp.transpose(memory, (0, 1, 3, 2)), norm, peak.T, read


def solution(mesh):
    in_specs = (
        P(None, "sp", None),
        P(None, "tp"),
        P(None, "tp"),
        P(None, "tp"),
        P(None, "tp"),
        P("tp"),
        P(None, "tp"),
        P(None, "sp", "tp"),
        P(None, "tp", None),
        P(None, "tp", None),
        P(None, "tp", "sp"),
        P(None, "tp"),
        P(None, "tp"),
        P("tp", "sp", None),
    )
    out_specs = (
        P(None, "tp", None, "sp"),
        P(None, "tp", "sp"),
        P(None, "tp"),
        P(None, ("sp", "tp")),
    )
    return jax.shard_map(body, mesh=mesh, in_specs=in_specs, out_specs=out_specs, check_vma=False)
```

time: 142 us -> 43.3 us (0.30)
  blocking collectives: 48.2 us -> 0 us
  Pallas kernels: 0 us -> 36.1 us
  matrix products: 33.6 us -> 0 us
  starting transfers between devices: 28.9 us -> 0 us
  waiting for transfers between devices: 10.3 us -> 0 us
  other arithmetic: 9.47 us -> 0 us
  local copies, waits for them, and re-layouts: 9.54 us -> 6.28 us
    pallas_call x0 -> x1, Pallas kernels: none -> 36.1 us  [body(): pl.pallas_call(kernel, out_shape=(jax.ShapeDtypeStruct((seqs, 2, 8, 64),...]
    dot_general x6 -> x0, matrix products: 33.6 us -> none  [the longest x1 10.7 us: project(): jnp.dot(flat_rows, key_weight, preferred_element_type=jnp.float32)]
    all_to_all x4 -> x0, starting transfers between devices: 22.9 us -> none  [the longest x1 9.52 us: copy_for_each(): return lax.all_to_all(copies, axis, split_axis=0, concat_axis=0, tiled=True)]
    pmax x2 -> x0, blocking collectives: 17.1 us -> none  [by_axis(): return functools.reduce(lax.pmax, axes, shard)]
    psum x2 -> x0, blocking collectives: 16.9 us -> none  [over_axes(): shard = lax.psum(shard, axis)]
    all_to_all x1 -> x0, blocking collectives: 14.2 us -> none  [sum_at_owner(): lax.all_to_all(in_blocks(shard, dim, devices), axis, 0, 0, tiled=True)]
    all_to_all x4 -> x0, waiting for transfers between devices: 10.3 us -> none  [the longest x1 7.78 us: sum_by_axis(): return jnp.sum(lax.all_to_all(own, far, 0, 0, tiled=True), axis=0)]
    ppermute x2 -> x0, starting transfers between devices: 5.99 us -> none  [the longest x1 4.7 us: with_halo(): before = lax.ppermute(last, axis, up)]
  transfers between devices with their start and end apart: 6 -> 0, of which waited for: 2 -> 0; matrix products, arithmetic and copies ran while one was open for 24% -> 0% of each run, Pallas kernels for 0% -> 0%
where the time goes in v1:
time: 43.3 us; the launch traced here: 43 us
  Pallas kernels  36.1 us (83%)
  local copies, waits for them, and re-layouts  6.28 us (15%)
  between operations  0.64 us (1%)
    pallas_call x1, Pallas kernels, body(): pl.pallas_call(kernel, out_shape=(jax.ShapeDtypeStruct((seqs, 2, 8, 64),...  36.1 us
    unnamed x4, local copies, waits for them, and re-layouts  4.98 us
    reshape x1, local copies, waits for them, and re-layouts, body(): forget_bias.reshape(2, 1)  1.3 us

profile of v1, /device:TPU:1, one launch (start us, length us, event | category | flops | bytes accessed | tf_op | source)
XLA Modules:
  0.0 43.0 jit_solution(11599993772486195121)
XLA Ops:
  0.6 1.3 %copy.18.fg_bias = f32[2,1]{1,0:T(2,128)} copy(f32[2,1]{0,1:T(1,128)} %bitcast.15) | data formatting | bytes 16 | tf_op jit(solution)/shard_map/reshape | solution.py:494
  1.9 36.1 %prompt_state.1 = (bf16[4,2,8,64]{3,2,1,0:T(8,128)(2,1)}, bf16[4,2,4]{2,1,0:T(2,128)(2,1)}, f32[2,4]{1,0:T(2,128)}, bf16[4,32]{1,0:T(4,128)(2,1)}) custom-call(bf16[4,512,4096]{2,1,0:T(8,128)(2,1)} %prompt.1, bf16[4096,128]{1,0:T(8,128)(2,1)} %key_w.1, bf16[4096,256]{1,0:T(8,128)(2,1)} %value_w.1, bf16[2,4096]{1,0:T(2,128)(2,1)} %bitcast.9, ...), custom_call_target="tpu_custom_call" | custom-call | tf_op jit(solution)/shard_map/prompt_state/pallas_call | solution.py:442
  38.0 1.3 %copy.23 = bf16[4,2,64,8]{2,3,1,0:T(8,128)(2,1)} copy(bf16[4,2,64,8]{2,3,1,0:T(8,128)(2,1)} %bitcast.8) | data formatting | bytes 16384
  39.3 1.2 %copy.24 = bf16[4,2,4]{2,1,0:T(2,128)(2,1)} copy(bf16[4,2,4]{2,1,0:T(2,128)(2,1)} %get-tuple-element.17) | data formatting | bytes 128
  40.6 1.2 %copy.25 = f32[4,2]{0,1:T(2,128)} copy(f32[4,2]{0,1:T(2,128)} %bitcast.14) | data formatting | bytes 64
  41.8 1.2 %copy.26 = bf16[4,32]{1,0:T(4,128)(2,1)} copy(bf16[4,32]{1,0:T(4,128)(2,1)} %get-tuple-element.19) | data formatting | bytes 512

commit v2 on v1

--- a/solution.py
+++ b/solution.py
@@ -29,10 +29,11 @@
 def kernel(
     prompt, key_w, value_w, in_w, fg_w, fg_bias, taps, extra, query, new_key, new_value,
     new_in, new_fg, out_w,
-    mem_out, norm_out, peak_out, read_out,
-    p_buf, wk_buf, wv_buf, wt_buf, hp_buf, r_buf, par_buf, mem_buf, e_buf,
+    packed,
+    p_buf, wk_buf, wv_buf, wt_buf, hp_buf, r_buf, tri_buf, par_buf, mem_buf, e_buf,
     h_send, h_recv, e_recv, m_recv, ow_recv, part_buf, part_recv,
-    w_sem, p_sem, hp_sem, ow_local, h_ssem, h_rsem, e_ssem, e_rsem, m_ssem, m_rsem,
+    in_v, fg_v, bias_v, taps_v, extra_v, query_v, key_v, value_v, nin_v, nfg_v,
+    w_sem, p_sem, hp_sem, small_sem, ow_local, h_ssem, h_rsem, e_ssem, e_rsem, m_ssem, m_rsem,
     ow_ssem, ow_rsem, o_ssem, o_rsem,
 ):
     seqs, length, width = p_buf.shape
@@ -48,14 +49,15 @@
     def tp_peer(d):
         return lax.rem(tp + d, tp_n)
 
-    @pl.loop(1, sp_n)
-    def _(d):
-        pl.semaphore_signal(barrier, inc=1, device_id=(sp_peer(d), tp), device_id_type=MESH_ID)
-
-    @pl.loop(1, tp_n)
-    def _(d):
-        pl.semaphore_signal(barrier, inc=1, device_id=(sp, tp_peer(d)), device_id_type=MESH_ID)
-
+    small_pairs = (
+        (in_w, in_v), (fg_w, fg_v), (fg_bias, bias_v), (taps, taps_v), (extra, extra_v),
+        (query, query_v), (new_key, key_v), (new_value, value_v), (new_in, nin_v),
+        (new_fg, nfg_v),
+    )
+    small_copies = [
+        pltpu.make_async_copy(src, dst, small_sem.at[i])
+        for i, (src, dst) in enumerate(small_pairs)
+    ]
     hp_copies = []
     for s in range(seqs):
         for side, row in ((0, 0), (1, length - 8)):
@@ -77,14 +79,7 @@
         p_copies.append(
             pltpu.make_async_copy(prompt.at[0, :, rows], p_buf.at[0, :, rows], p_sem.at[0, c])
         )
-    for c in range(CHUNKS):
-        for copy in w_copies[c]:
-            copy.start()
-        p_copies[c].start()
-        if c == 0:
-            for copy in hp_copies:
-                copy.start()
-    s_copies = [None]
+    s_copies = [p_copies]
     for s in range(1, seqs):
         group = []
         for c in range(CHUNKS):
@@ -92,9 +87,36 @@
             group.append(
                 pltpu.make_async_copy(prompt.at[s, rows, :], p_buf.at[s, rows, :], p_sem.at[s, c])
             )
-        for copy in group:
+        s_copies.append(group)
+
+    def start(copies):
+        for copy in copies:
             copy.start()
-        s_copies.append(group)
+
+    def finished(copies):
+        for copy in copies:
+            copy.wait()
+
+    start(small_copies[:2])
+    start(w_copies[0])
+    start(p_copies[0:1])
+    start(small_copies[2:])
+    start(w_copies[1])
+    start(p_copies[1:2])
+    start(hp_copies)
+
+    @pl.loop(1, sp_n)
+    def _(d):
+        pl.semaphore_signal(barrier, inc=1, device_id=(sp_peer(d), tp), device_id_type=MESH_ID)
+
+    @pl.loop(1, tp_n)
+    def _(d):
+        pl.semaphore_signal(barrier, inc=1, device_id=(sp, tp_peer(d)), device_id_type=MESH_ID)
+
+    tri_buf[...] = (
+        lax.broadcasted_iota(jnp.int32, (length, length), 0)
+        > lax.broadcasted_iota(jnp.int32, (length, length), 1)
+    ).astype(F32).astype(BF16)
 
     lane = lax.broadcasted_iota(jnp.int32, (1, 128), 1)
     first_head = lane < 64
@@ -102,38 +124,16 @@
     def halves(left, right):
         return jnp.where(first_head, left, right)
 
-    for s in range(seqs):
-        rows = pl.ds(s, 1)
-        par_buf[0, rows, :] = jnp.concatenate(
-            [query[s, 0:1, :].astype(F32), query[s, 1:2, :].astype(F32)], axis=1
-        )
-        par_buf[1, rows, :] = jnp.concatenate(
-            [new_key[s, 0:1, :].astype(F32), new_key[s, 1:2, :].astype(F32)], axis=1
-        )
-        par_buf[2, rows, :] = halves(new_in[0:1, s : s + 1], new_in[1:2, s : s + 1])
-        par_buf[3, rows, :] = halves(new_fg[0:1, s : s + 1], new_fg[1:2, s : s + 1])
-    tap_cols = jnp.transpose(
-        jnp.concatenate([taps[...].astype(F32), jnp.zeros((5, 128), F32)], axis=0)
-    )
-    q_cols = jnp.transpose(
-        jnp.concatenate([par_buf[0, 0:4, :], jnp.zeros((4, 128), F32)], axis=0)
-    )
-    gate_rows = jnp.concatenate(
-        [
-            in_w[...].astype(F32), jnp.zeros((6, width), F32),
-            fg_w[...].astype(F32), jnp.zeros((6, width), F32),
-        ],
-        axis=0,
-    )
-    wt_buf[0:KEY0, :] = gate_rows.astype(BF16)
-
-    for c in range(CHUNKS):
-        cols = pl.ds(c * step, step)
-        for copy in w_copies[c]:
-            copy.wait()
+    def chunk_of(c):
+        return pl.ds(c * step, step)
+
+    def turn(c):
+        cols = chunk_of(c)
         wt_buf[KEY0:VAL0, cols] = jnp.transpose(wk_buf[cols, :])
         wt_buf[VAL0:, cols] = jnp.transpose(wv_buf[cols, :])
-        p_copies[c].wait()
+
+    def chunk_dot(c):
+        cols = chunk_of(c)
         part = lax.dot_general(
             wt_buf[:, cols], p_buf[0, :, cols], NT, preferred_element_type=F32
         )
@@ -142,8 +142,38 @@
         else:
             r_buf[0] = r_buf[0] + part
 
-    for copy in hp_copies:
-        copy.wait()
+    finished(small_copies[:2])
+    gate_rows = jnp.concatenate(
+        [
+            in_v[...].astype(F32), jnp.zeros((6, width), F32),
+            fg_v[...].astype(F32), jnp.zeros((6, width), F32),
+        ],
+        axis=0,
+    )
+    wt_buf[0:KEY0, :] = gate_rows.astype(BF16)
+    finished(w_copies[0])
+    start(w_copies[2])
+    turn(0)
+    finished(p_copies[0:1])
+    start(p_copies[2:3])
+    finished(w_copies[1])
+    start(w_copies[3])
+    chunk_dot(0)
+    turn(1)
+    finished(p_copies[1:2])
+    start(p_copies[3:4])
+    finished(w_copies[2])
+    start(s_copies[1][:2])
+    chunk_dot(1)
+    turn(2)
+    finished(p_copies[2:3])
+    start(s_copies[1][2:])
+    finished(w_copies[3])
+    finished(hp_copies)
+    start(s_copies[2][:2])
+    chunk_dot(2)
+    turn(3)
+
     edge = jnp.dot(hp_buf[...], wk_buf[...], preferred_element_type=F32).astype(BF16).astype(F32)
     zero4 = jnp.zeros((4, 128), F32)
     h_send[0] = jnp.concatenate(
@@ -154,18 +184,6 @@
     )
 
     pl.semaphore_wait(barrier, sp_n - 1 + tp_n - 1)
-
-    cols_of = out_w.shape[2] // sp_n
-
-    def ow_slot(ref):
-        return ref.at[sp // 8, :, lax.rem(sp, 8)]
-
-    def ow_cols(j):
-        return out_w.at[:, :, pl.ds(pl.multiple_of(j * cols_of, cols_of), cols_of)]
-
-    own_ow = pltpu.make_async_copy(ow_cols(sp), ow_slot(ow_recv), ow_local)
-    own_ow.start()
-
     halo_copies = []
     for side, d in ((0, 1), (1, sp_n - 1)):
         copy = pltpu.make_async_remote_copy(
@@ -179,17 +197,38 @@
         copy.start()
         halo_copies.append(copy)
 
-    @pl.loop(1, sp_n)
-    def _(d):
-        j = sp_peer(d)
-        pltpu.make_async_remote_copy(
-            src_ref=ow_cols(j),
-            dst_ref=ow_slot(ow_recv),
-            send_sem=ow_ssem,
-            recv_sem=ow_rsem,
-            device_id=(j, tp),
-            device_id_type=MESH_ID,
-        ).start()
+    finished(p_copies[3:4])
+    start(s_copies[2][2:])
+    chunk_dot(3)
+
+    finished(small_copies[2:])
+    for s in range(seqs):
+        rows = pl.ds(s, 1)
+        par_buf[0, rows, :] = jnp.concatenate(
+            [query_v[s, 0:1, :].astype(F32), query_v[s, 1:2, :].astype(F32)], axis=1
+        )
+        par_buf[1, rows, :] = jnp.concatenate(
+            [key_v[s, 0:1, :].astype(F32), key_v[s, 1:2, :].astype(F32)], axis=1
+        )
+        par_buf[2, rows, :] = halves(nin_v[0:1, s : s + 1], nin_v[1:2, s : s + 1])
+        par_buf[3, rows, :] = halves(nfg_v[0:1, s : s + 1], nfg_v[1:2, s : s + 1])
+    tap_cols = jnp.transpose(
+        jnp.concatenate([taps_v[...].astype(F32), jnp.zeros((5, 128), F32)], axis=0)
+    )
+    q_cols = jnp.transpose(
+        jnp.concatenate([par_buf[0, 0:4, :], jnp.zeros((4, 128), F32)], axis=0)
+    )
+    bias_col = jnp.where(
+        lax.broadcasted_iota(jnp.int32, (2, 1), 0) == 0, bias_v[0], bias_v[1]
+    )
+
+    cols_of = out_w.shape[2] // sp_n
+
+    def ow_slot(ref):
+        return ref.at[sp // 8, :, lax.rem(sp, 8)]
+
+    def ow_cols(j):
+        return out_w.at[:, :, pl.ds(pl.multiple_of(j * cols_of, cols_of), cols_of)]
 
     def edges():
         for copy in halo_copies:
@@ -204,24 +243,22 @@
     def slot_rows(s):
         return pl.ds(pl.multiple_of((s * sp_n + sp) * 8, 8), 8)
 
+    def rows_of(x):
+        parts = [part.astype(F32) for part in three_parts(x)]
+        return jnp.concatenate(parts + [jnp.zeros((10, length), F32)], axis=0).astype(BF16)
+
     def finish(s, before, after):
-        buf = s % 2
-        in_pre = r_buf[buf, 0:2, :].astype(BF16).astype(F32)
-        fg_pre = r_buf[buf, 8:10, :].astype(BF16).astype(F32)
-        log_f = log_sigmoid(fg_pre + fg_bias[...]) + extra[s]
-        later = jnp.where(pos < length - 1, pltpu.roll(log_f, length - 1, 1), 0.0)
-        shift = 1
-        while shift < length:
-            later = later + jnp.where(
-                pos < length - shift, pltpu.roll(later, length - shift, 1), 0.0
-            )
-            shift *= 2
+        in_pre = r_buf[s, 0:2, :].astype(BF16).astype(F32)
+        fg_pre = r_buf[s, 8:10, :].astype(BF16).astype(F32)
+        log_f = log_sigmoid(fg_pre + bias_col) + extra_v[s]
+        sums = jnp.dot(rows_of(log_f), tri_buf[...], preferred_element_type=F32)
+        later = sums[0:2] + sums[2:4] + sums[4:6]
         total = later[:, 0:1] + log_f[:, 0:1]
         gate = in_pre + later
         top = jnp.max(gate, axis=1, keepdims=True)
         scale = jnp.exp(gate - top)
 
-        key = r_buf[buf, KEY0:VAL0, :].astype(BF16).astype(F32)
+        key = r_buf[s, KEY0:VAL0, :].astype(BF16).astype(F32)
         earlier = jnp.where(pos == 0, before[:, s : s + 1], pltpu.roll(key, 1, 1))
         coming = jnp.where(pos == length - 1, after[:, s : s + 1], pltpu.roll(key, length - 1, 1))
         mixed = tap_cols[:, 0:1] * earlier + tap_cols[:, 1:2] * key + tap_cols[:, 2:3] * coming
@@ -234,7 +271,7 @@
             ],
             axis=0,
         )
-        value = r_buf[buf, VAL0:, :].astype(BF16).astype(F32)
+        value = r_buf[s, VAL0:, :].astype(BF16).astype(F32)
         weighted = jnp.concatenate(
             [
                 (value[0:128] * scale[0:1]).astype(BF16),
@@ -243,10 +280,6 @@
             axis=0,
         )
 
-        def rows_of(x):
-            parts = [part.astype(F32) for part in three_parts(x)]
-            return jnp.concatenate(parts + [jnp.zeros((10, length), F32)], axis=0).astype(BF16)
-
         norm_parts = lax.dot_general(rows_of(scale), key_rows, NT, preferred_element_type=F32)
         num_parts = lax.dot_general(rows_of(along), weighted, NT, preferred_element_type=F32)
         outer = lax.dot_general(weighted, key_rows, NT, preferred_element_type=F32)
@@ -261,7 +294,7 @@
         num_a = halves(num0, pltpu.roll(num1, 64, 1))
         num_b = halves(pltpu.roll(num0, 64, 1), num1)
 
-        fresh = new_value[s].astype(F32)
+        fresh = value_v[s].astype(F32)
         spread = jnp.concatenate([fresh, jnp.zeros((2, 120), F32)], axis=1)
         left = pltpu.roll(spread, 8 * lax.rem(sp, 8), 1)
         fresh_row = halves(left[0:1], pltpu.roll(left[1:2], 64, 1))
@@ -284,6 +317,7 @@
         e_recv[slot_rows(s), :] = tile
         m_recv[slot_rows(s), :] = mem_buf[pl.ds(128 * s + my_rows, 8), :]
 
+    def send(s):
         @pl.loop(1, sp_n)
         def _(d):
             pltpu.make_async_remote_copy(
@@ -307,15 +341,46 @@
                 device_id_type=MESH_ID,
             ).start()
 
-    before = after = None
-    for s in range(1, seqs):
-        for copy in s_copies[s]:
-            copy.wait()
-        if s == 1:
-            before, after = edges()
-        r_buf[s % 2] = lax.dot_general(wt_buf[...], p_buf[s], NT, preferred_element_type=F32)
-        finish(s - 1, before, after)
-    finish(seqs - 1, before, after)
+    def half_dot(s, half):
+        rows = pl.ds(half * (length // 2), length // 2)
+        r_buf[s, :, rows] = lax.dot_general(
+            wt_buf[...], p_buf[s, rows, :], NT, preferred_element_type=F32
+        )
+
+    finished(s_copies[1])
+    start(s_copies[3])
+    half_dot(1, 0)
+    half_dot(1, 1)
+    own_ow = pltpu.make_async_copy(ow_cols(sp), ow_slot(ow_recv), ow_local)
+    own_ow.start()
+
+    @pl.loop(1, sp_n)
+    def _(d):
+        j = sp_peer(d)
+        pltpu.make_async_remote_copy(
+            src_ref=ow_cols(j),
+            dst_ref=ow_slot(ow_recv),
+            send_sem=ow_ssem,
+            recv_sem=ow_rsem,
+            device_id=(j, tp),
+            device_id_type=MESH_ID,
+        ).start()
+
+    finished(s_copies[2])
+    before, after = edges()
+    half_dot(2, 0)
+    finish(0, before, after)
+    half_dot(2, 1)
+    send(0)
+    finished(s_copies[3])
+    half_dot(3, 0)
+    finish(1, before, after)
+    finish(2, before, after)
+    half_dot(3, 1)
+    send(1)
+    send(2)
+    finish(3, before, after)
+    send(3)
 
     def take(ref, sem, count):
         view = ref.at[pl.ds(0, count), :]
@@ -367,11 +432,9 @@
         read_a = (old_scale * num_a + fresh_scale * fresh_a) / denom
         read_b = (old_scale * num_b + fresh_scale * fresh_b) / denom
         reads.append(jnp.concatenate([read_a, read_b], axis=1))
-        mine = pltpu.roll(norm, lax.rem(128 - 4 * sp, 128), 1).astype(BF16)
-        norm_out[s, 0:1, :] = mine[:, 0:4]
-        norm_out[s, 1:2, :] = mine[:, 64:68]
-        peak_out[0:1, s : s + 1] = peak[:, 0:1]
-        peak_out[1:2, s : s + 1] = peak[:, 64:65]
+        mine = pltpu.roll(norm, lax.rem(128 - 4 * sp, 128), 1)
+        packed[32 + s : 33 + s, :] = mine
+        packed[36 + s : 37 + s, :] = peak
 
     ow_words = pltpu.make_async_copy(
         out_w.at[:, :, pl.ds(0, cols_of * (sp_n - 1))],
@@ -403,8 +466,7 @@
         for i in range(sp_n):
             base = (s * sp_n + i) * 8
             memory = memory + factors[s][i : i + 1] * m_recv[base : base + 8, :]
-        mem_out[s, 0] = memory[:, 0:64].astype(BF16)
-        mem_out[s, 1] = memory[:, 64:128].astype(BF16)
+        packed[8 * s : 8 * s + 8, :] = memory
 
     view = part_recv.at[pl.ds(0, tp_n - 1)]
     pltpu.make_async_copy(view, view, o_rsem).wait()
@@ -412,7 +474,7 @@
     for i in range(1, tp_n):
         whole = whole + part_recv[i]
     turned = pltpu.roll(whole, lax.rem(cols_of - 32 * tp, cols_of), 1)
-    read_out[...] = turned[0:4, 0:32].astype(BF16)
+    packed[40:48, :] = turned[:, 0:128]
 
     for copy in halo_copies:
         copy.wait_send()
@@ -425,6 +487,21 @@
         take(e_recv, e_ssem.at[s], 8 * (sp_n - 1))
         take(m_recv, m_ssem.at[s], 8 * (sp_n - 1))
     pltpu.make_async_copy(view, view, o_ssem).wait()
+
+
+def unpack(packed, mem_out, norm_out, peak_out, read_out):
+    seqs = mem_out.shape[0]
+    for s in range(seqs):
+        rows = packed[8 * s : 8 * s + 8, :]
+        mem_out[s, 0] = rows[:, 0:64].astype(BF16)
+        mem_out[s, 1] = rows[:, 64:128].astype(BF16)
+        norm = packed[32 + s : 33 + s, :]
+        norm_out[s, 0:1, :] = norm[:, 0:4].astype(BF16)
+        norm_out[s, 1:2, :] = norm[:, 64:68].astype(BF16)
+        peak = packed[36 + s : 37 + s, :]
+        peak_out[0:1, s : s + 1] = peak[:, 0:1]
+        peak_out[1:2, s : s + 1] = peak[:, 64:65]
+    read_out[...] = packed[40:44, 0:32].astype(BF16)
 
 
 def body(
@@ -439,23 +516,19 @@
     any_spec = pl.BlockSpec(memory_space=pl.ANY)
     vmem = pl.BlockSpec(memory_space=pltpu.VMEM)
     dma = pltpu.SemaphoreType.DMA
-    memory, norm, peak, read = pl.pallas_call(
+    packed = pl.pallas_call(
         kernel,
-        out_shape=(
-            jax.ShapeDtypeStruct((seqs, 2, 8, 64), BF16),
-            jax.ShapeDtypeStruct((seqs, 2, 4), BF16),
-            jax.ShapeDtypeStruct((2, seqs), F32),
-            jax.ShapeDtypeStruct((seqs, 32), BF16),
-        ),
-        in_specs=[any_spec] * 3 + [vmem] * 10 + [any_spec],
-        out_specs=(vmem,) * 4,
+        out_shape=pltpu.VMEM((48, 128), F32),
+        in_specs=[any_spec] * 14,
+        out_specs=vmem,
         scratch_shapes=[
             pltpu.VMEM((seqs, length, width), BF16),
             pltpu.VMEM((width, 128), BF16),
             pltpu.VMEM((width, 256), BF16),
             pltpu.VMEM((400, width), BF16),
             pltpu.VMEM((64, width), BF16),
-            pltpu.VMEM((2, 400, length), F32),
+            pltpu.VMEM((seqs, 400, length), F32),
+            pltpu.VMEM((length, length), BF16),
             pltpu.VMEM((4, 8, 128), F32),
             pltpu.VMEM((seqs * 128, 128), F32),
             pltpu.VMEM((seqs * 8, 128), F32),
@@ -466,9 +539,20 @@
             pltpu.VMEM((2, 2, 8, 8, cols_of), BF16),
             pltpu.VMEM((8, cols_of), F32),
             pltpu.VMEM((tp_n, 8, cols_of), F32),
+            pltpu.VMEM((2, width), BF16),
+            pltpu.VMEM((2, width), BF16),
+            pltpu.SMEM((2,), F32),
+            pltpu.VMEM((3, 128), BF16),
+            pltpu.VMEM((seqs, 2, length), F32),
+            pltpu.VMEM((seqs, 2, 64), BF16),
+            pltpu.VMEM((seqs, 2, 64), BF16),
+            pltpu.VMEM((seqs, 2, 8), BF16),
+            pltpu.VMEM((2, seqs), F32),
+            pltpu.VMEM((2, seqs), F32),
             dma((2, CHUNKS)),
             dma((seqs, CHUNKS)),
             dma((2 * seqs,)),
+            dma((10,)),
             dma,
             dma((2,)),
             dma((2,)),
@@ -491,7 +575,7 @@
         value_weight,
         input_gate_weight.T,
         forget_gate_weight.T,
-        forget_bias.reshape(2, 1),
+        forget_bias,
         key_taps,
         jnp.transpose(extra_decay, (0, 2, 1)),
         new_query,
@@ -501,6 +585,19 @@
         new_forget_gate.T,
         out_weight,
     )
+    memory, norm, peak, read = pl.pallas_call(
+        unpack,
+        out_shape=(
+            jax.ShapeDtypeStruct((seqs, 2, 8, 64), BF16),
+            jax.ShapeDtypeStruct((seqs, 2, 4), BF16),
+            jax.ShapeDtypeStruct((2, seqs), F32),
+            jax.ShapeDtypeStruct((seqs, 32), BF16),
+        ),
+        in_specs=[vmem],
+        out_specs=(vmem,) * 4,
+        compiler_params=pltpu.CompilerParams(vmem_limit_bytes=1024 * 1024),
+        name="unpack",
+    )(packed)
     return jnp.transpose(memory, (0, 1, 3, 2)), norm, peak.T, read
 
 

time: 43.3 us -> 33.3 us (0.77)
  local copies, waits for them, and re-layouts: 6.28 us -> 0 us
  Pallas kernels: 36.1 us -> 32.5 us
    unnamed x4 -> x0, local copies, waits for them, and re-layouts: 4.98 us -> none
    pallas_call x1 -> x2, Pallas kernels: 36.1 us -> 32.5 us  [the longest x1 31.8 us: body(): pl.pallas_call(kernel, out_shape=pltpu.VMEM((48, 128), F32), in_specs=[an...]
    reshape x1 -> x0, local copies, waits for them, and re-layouts: 1.3 us -> none  [body(): forget_bias.reshape(2, 1)]
where the time goes in v2:
time: 33.3 us; the launch traced here: 33.1 us
  Pallas kernels  32.5 us (98%)
  between operations  0.64 us (2%)
    pallas_call x1, Pallas kernels, body(): pl.pallas_call(kernel, out_shape=pltpu.VMEM((48, 128), F32), in_specs=[an...  31.8 us
    pallas_call x1, Pallas kernels, body(): pl.pallas_call(unpack, out_shape=(jax.ShapeDtypeStruct((seqs, 2, 8, 64),...  0.7 us

profile of v2, /device:TPU:1, one launch (start us, length us, event | category | flops | bytes accessed | tf_op | source)
XLA Modules:
  0.0 33.1 jit_solution(13320494601875188995)
XLA Ops:
  0.6 31.8 %prompt_state.1.packed = f32[48,128]{1,0:T(8,128)S(1)} custom-call(bf16[4,512,4096]{2,1,0:T(8,128)(2,1)} %prompt.1, bf16[4096,128]{1,0:T(8,128)(2,1)} %key_w.1, bf16[4096,256]{1,0:T(8,128)(2,1)} %value_w.1, bf16[2,4096]{1,0:T(2,128)(2,1)} %bitcast.7, bf16[2,4096]{1,0:T(2,128)(2,1)} %bitcast.8, f32[2]{0:T(128)} %fg_bias.1, bf16[3,128]{1,0:T(4,128)(2,1)} %taps.1, ...), custom_call_target="tpu_custom_call" | custom-call | tf_op jit(solution)/shard_map/prompt_state/pallas_call | solution.py:519
  32.4 0.7 %unpack.1 = (bf16[4,2,8,64]{3,2,1,0:T(8,128)(2,1)}, bf16[4,2,4]{2,1,0:T(2,128)(2,1)}, f32[2,4]{1,0:T(2,128)}, bf16[4,32]{1,0:T(4,128)(2,1)}) custom-call(f32[48,128]{1,0:T(8,128)S(1)} %prompt_state.1.packed), custom_call_target="tpu_custom_call" | custom-call | tf_op jit(solution)/shard_map/unpack/pallas_call | solution.py:588

commit v3 on v2

v3 whole, which is shorter than its diff:
```python
import jax
import jax.numpy as jnp
from jax import lax
from jax.experimental import pallas as pl
from jax.experimental.pallas import tpu as pltpu
from jax.sharding import PartitionSpec as P

MESH_ID = pl.DeviceIdType.MESH
F32 = jnp.float32
BF16 = jnp.bfloat16
NT = (((1,), (1,)), ((), ()))
KEY0 = 16
VAL0 = 144
CHUNKS = 4


def log_sigmoid(x):
    return jnp.minimum(x, 0.0) - jnp.log1p(jnp.exp(-jnp.abs(x)))


def three_parts(x):
    high = x.astype(BF16)
    rest = x - high.astype(F32)
    middle = rest.astype(BF16)
    low = (rest - middle.astype(F32)).astype(BF16)
    return high, middle, low


def kernel(
    prompt, key_w, value_w, in_w, fg_w, fg_bias, taps, extra, query, new_key, new_value,
    new_in, new_fg, out_w,
    packed,
    p_buf, wk_buf, wv_buf, wt_buf, hp_buf, r_buf, tri_buf, par_buf, mem_buf, e_buf,
    h_send, h_recv, e_recv, m_recv, ow_recv, part_buf, part_recv, f_buf, f_recv, lhs_buf, key_buf,
    along_buf, suf_buf, ow_buf, col_buf,
    in_v, fg_v, bias_v, taps_v, extra_v, query_v, key_v, value_v, nin_v, nfg_v,
    w_sem, p_sem, hp_sem, small_sem, ow_local, h_ssem, h_rsem, e_ssem, e_rsem, m_ssem, m_rsem,
    ow_ssem, ow_rsem, o_ssem, o_rsem, f_ssem, f_rsem,
):
    seqs, length, width = p_buf.shape
    sp_n, tp_n = lax.axis_size("sp"), lax.axis_size("tp")
    sp, tp = lax.axis_index("sp"), lax.axis_index("tp")
    step = width // CHUNKS

    barrier = pltpu.get_barrier_semaphore()

    def sp_peer(d):
        return lax.rem(sp + d, sp_n)

    def tp_peer(d):
        return lax.rem(tp + d, tp_n)

    small_pairs = (
        (in_w, in_v), (fg_w, fg_v), (fg_bias, bias_v), (taps, taps_v), (extra, extra_v),
        (query, query_v), (new_key, key_v), (new_value, value_v), (new_in, nin_v),
        (new_fg, nfg_v),
    )
    small_copies = [
        pltpu.make_async_copy(src, dst, small_sem.at[i])
        for i, (src, dst) in enumerate(small_pairs)
    ]
    hp_copies = []
    for s in range(seqs):
        for side, row in ((0, 0), (1, length - 8)):
            g = 2 * s + side
            hp_copies.append(
                pltpu.make_async_copy(
                    prompt.at[s, pl.ds(row, 8), :], hp_buf.at[pl.ds(8 * g, 8), :], hp_sem.at[g]
                )
            )
    wk_copies = [
        pltpu.make_async_copy(key_w.at[rows, :], wk_buf.at[rows, :], w_sem.at[0, i])
        for i, rows in enumerate((pl.ds(0, width // 2), pl.ds(width // 2, width // 2)))
    ]
    w_copies, p_copies = [], []
    for c in range(CHUNKS):
        rows = pl.ds(c * step, step)
        w_copies.append(
            pltpu.make_async_copy(value_w.at[rows, :], wv_buf.at[rows, :], w_sem.at[1, c])
        )
        p_copies.append(
            pltpu.make_async_copy(prompt.at[0, :, rows], p_buf.at[0, :, rows], p_sem.at[0, c])
        )
    s_copies = [p_copies]
    for s in range(1, seqs):
        group = []
        for c in range(CHUNKS):
            cols = pl.ds(c * step, step)
            group.append(
                pltpu.make_async_copy(prompt.at[s, :, cols], p_buf.at[s, :, cols], p_sem.at[s, c])
            )
        s_copies.append(group)

    def start(copies):
        for copy in copies:
            copy.start()

    def finished(copies):
        for copy in copies:
            copy.wait()

    start(wk_copies)
    start(hp_copies)
    start(w_copies[:1])
    start(p_copies[:1])
    start(small_copies)
    start(w_copies[1:2])
    start(p_copies[1:2])

    @pl.loop(1, sp_n)
    def _(d):
        pl.semaphore_signal(barrier, inc=1, device_id=(sp_peer(d), tp), device_id_type=MESH_ID)

    @pl.loop(1, tp_n)
    def _(d):
        pl.semaphore_signal(barrier, inc=1, device_id=(sp, tp_peer(d)), device_id_type=MESH_ID)

    tri_buf[...] = (
        lax.broadcasted_iota(jnp.int32, (length, length), 0)
        > lax.broadcasted_iota(jnp.int32, (length, length), 1)
    ).astype(F32).astype(BF16)

    lane = lax.broadcasted_iota(jnp.int32, (1, 128), 1)
    first_head = lane < 64

    def halves(left, right):
        return jnp.where(first_head, left, right)

    def chunk_of(c):
        return pl.ds(c * step, step)

    def turn(c):
        cols = chunk_of(c)
        wt_buf[VAL0:, cols] = jnp.transpose(wv_buf[cols, :])

    def chunk_dot(s, c):
        cols = chunk_of(c)
        part = lax.dot_general(
            wt_buf[:, cols], p_buf[s, :, cols], NT, preferred_element_type=F32
        )
        if c == 0:
            r_buf[s] = part
        else:
            r_buf[s] = r_buf[s] + part

    finished(wk_copies)
    start(w_copies[2:])
    start(p_copies[2:])
    for c in range(CHUNKS):
        cols = chunk_of(c)
        wt_buf[KEY0:VAL0, cols] = jnp.transpose(wk_buf[cols, :])
    finished(hp_copies)

    edge = jnp.dot(hp_buf[...], wk_buf[...], preferred_element_type=F32).astype(BF16).astype(F32)
    zero4 = jnp.zeros((4, 128), F32)
    h_send[0] = jnp.concatenate(
        [edge[16 * s + 15 : 16 * s + 16] for s in range(seqs)] + [zero4], axis=0
    )
    h_send[1] = jnp.concatenate(
        [edge[16 * s : 16 * s + 1] for s in range(seqs)] + [zero4], axis=0
    )

    finished(small_copies)
    gate_rows = jnp.concatenate(
        [
            in_v[...].astype(F32), jnp.zeros((6, width), F32),
            fg_v[...].astype(F32), jnp.zeros((6, width), F32),
        ],
        axis=0,
    )
    wt_buf[0:KEY0, :] = gate_rows.astype(BF16)
    finished(w_copies[:1])
    start(s_copies[1][:2])
    turn(0)
    finished(p_copies[:1])
    finished(w_copies[1:2])
    start(s_copies[1][2:])
    chunk_dot(0, 0)
    turn(1)
    pl.semaphore_wait(barrier, sp_n - 1 + tp_n - 1)
    halo_copies = []
    for side, d in ((0, 1), (1, sp_n - 1)):
        copy = pltpu.make_async_remote_copy(
            src_ref=h_send.at[side],
            dst_ref=h_recv.at[side],
            send_sem=h_ssem.at[side],
            recv_sem=h_rsem.at[side],
            device_id=(sp_peer(d), tp),
            device_id_type=MESH_ID,
        )
        copy.start()
        halo_copies.append(copy)

    finished(p_copies[1:2])
    finished(w_copies[2:3])
    chunk_dot(0, 1)
    turn(2)
    finished(p_copies[2:3])
    finished(w_copies[3:])
    start(s_copies[2][:2])
    chunk_dot(0, 2)
    turn(3)

    for s in range(seqs):
        rows = pl.ds(s, 1)
        par_buf[0, rows, :] = jnp.concatenate(
            [query_v[s, 0:1, :].astype(F32), query_v[s, 1:2, :].astype(F32)], axis=1
        )
        par_buf[1, rows, :] = jnp.concatenate(
            [key_v[s, 0:1, :].astype(F32), key_v[s, 1:2, :].astype(F32)], axis=1
        )
        par_buf[2, rows, :] = halves(nin_v[0:1, s : s + 1], nin_v[1:2, s : s + 1])
        par_buf[3, rows, :] = halves(nfg_v[0:1, s : s + 1], nfg_v[1:2, s : s + 1])
        fresh = value_v[s].astype(F32)
        spread = jnp.concatenate([fresh, jnp.zeros((2, 120), F32)], axis=1)
        left = pltpu.roll(spread, 8 * lax.rem(sp, 8), 1)
        fresh_row = halves(left[0:1], pltpu.roll(left[1:2], 64, 1))
        f_buf[s : s + 1, :] = jnp.where(sp < 8, fresh_row, 0.0)
        f_buf[4 + s : 5 + s, :] = jnp.where(sp < 8, 0.0, fresh_row)
    col_buf[:, 0:8] = jnp.transpose(
        jnp.concatenate(
            [taps_v[...].astype(F32), jnp.zeros((1, 128), F32), par_buf[0, 0:4, :]], axis=0
        )
    )

    bias_col = jnp.where(
        lax.broadcasted_iota(jnp.int32, (2, 1), 0) == 0, bias_v[0], bias_v[1]
    )

    cols_of = out_w.shape[2] // sp_n

    def ow_slot(ref):
        return ref.at[sp // 8, :, lax.rem(sp, 8)]

    def ow_cols(j):
        return out_w.at[:, :, pl.ds(pl.multiple_of(j * cols_of, cols_of), cols_of)]

    pos = lax.broadcasted_iota(jnp.int32, (1, length), 1)
    my_rows = pl.multiple_of(8 * sp, 8)
    my_tile = pl.multiple_of(8 * sp, 8)

    def slot_rows(s, size):
        return pl.ds(pl.multiple_of((s * sp_n + sp) * size, size), size)

    def rows_of(x):
        parts = [part.astype(F32) for part in three_parts(x)]
        return jnp.concatenate(parts + [jnp.zeros((10, length), F32)], axis=0).astype(BF16)

    def joined(x, h):
        return x[h : h + 1] + x[2 + h : 3 + h] + x[4 + h : 5 + h]

    def suffix(s):
        fg_pre = r_buf[s, 8:10, :].astype(BF16).astype(F32)
        log_f = log_sigmoid(fg_pre + bias_col) + extra_v[s]
        sums = jnp.dot(rows_of(log_f), tri_buf[...], preferred_element_type=F32)
        later = sums[0:2] + sums[2:4] + sums[4:6]
        suf_buf[s, 0:2, :] = later
        suf_buf[s, 2:4, :] = jnp.broadcast_to(later[:, 0:1] + log_f[:, 0:1], (2, length))

    def keys(s):
        key = r_buf[s, KEY0:VAL0, :].astype(BF16).astype(F32)
        earlier = jnp.where(pos == 0, col_buf[:, 8 + s : 9 + s], pltpu.roll(key, 1, 1))
        coming = jnp.where(
            pos == length - 1, col_buf[:, 16 + s : 17 + s], pltpu.roll(key, length - 1, 1)
        )
        mixed = col_buf[:, 0:1] * earlier + col_buf[:, 1:2] * key + col_buf[:, 2:3] * coming
        key_rows = (mixed * jax.nn.sigmoid(mixed) * 0.125).astype(BF16)
        key_buf[s] = key_rows
        prod = key_rows.astype(F32) * col_buf[:, 4 + s : 5 + s]
        along = jnp.concatenate(
            [
                jnp.sum(prod[0:64], axis=0, keepdims=True),
                jnp.sum(prod[64:128], axis=0, keepdims=True),
            ],
            axis=0,
        )
        along_buf[s] = rows_of(along)

    def weigh(s):
        in_pre = r_buf[s, 0:2, :].astype(BF16).astype(F32)
        gate = in_pre + suf_buf[s, 0:2, :]
        top = jnp.max(gate, axis=1, keepdims=True)
        scale = jnp.exp(gate - top)
        lhs_buf[s, 0:16, :] = rows_of(scale)
        for h in range(2):
            value = r_buf[s, VAL0 + 128 * h : VAL0 + 128 * (h + 1), :].astype(BF16).astype(F32)
            lhs_buf[s, 16 + 128 * h : 144 + 128 * h, :] = (value * scale[h : h + 1]).astype(BF16)
        total = suf_buf[s, 2:4, 0:1]
        row = jnp.where(
            lax.rem(lane, 64) < 32,
            halves(total[0:1], total[1:2]),
            halves(top[0:1], top[1:2]),
        )
        e_buf[4 * s + 3 : 4 * s + 4, :] = row

    def outer(s):
        num_parts = lax.dot_general(
            along_buf[s], lhs_buf[s, 16:, :], NT, preferred_element_type=F32
        )
        both = lax.dot_general(lhs_buf[s], key_buf[s], NT, preferred_element_type=F32)
        num0 = joined(num_parts, 0)[:, 0:128]
        num1 = joined(num_parts, 1)[:, 128:256]
        e_buf[4 * s : 4 * s + 1, :] = halves(joined(both, 0), joined(both, 1))
        e_buf[4 * s + 1 : 4 * s + 2, :] = halves(num0, pltpu.roll(num1, 64, 1))
        e_buf[4 * s + 2 : 4 * s + 3, :] = halves(pltpu.roll(num0, 64, 1), num1)
        mem_buf[pl.ds(128 * s, 128), :] = halves(both[16:144], both[144:272])

    z, x = sp // 4, lax.rem(sp, 4)
    offsets = sorted(
        ((dz, dx) for dz in range(4) for dx in range(4) if dz or dx),
        key=lambda o: -(min(o[0], 4 - o[0]) + min(o[1], 4 - o[1])),
    )
    peers = [lax.rem(z + dz, 4) * 4 + lax.rem(x + dx, 4) for dz, dx in offsets]

    def send_sums(s):
        e_recv[slot_rows(s, 4), :] = e_buf[4 * s : 4 * s + 4, :]
        for j in peers:
            pltpu.make_async_remote_copy(
                src_ref=e_buf.at[pl.ds(4 * s, 4), :],
                dst_ref=e_recv.at[slot_rows(s, 4), :],
                send_sem=e_ssem.at[s],
                recv_sem=e_rsem.at[s],
                device_id=(j, tp),
                device_id_type=MESH_ID,
            ).start()

    def send_memory(s):
        m_recv[slot_rows(s, 8), :] = mem_buf[pl.ds(128 * s + my_rows, 8), :]
        for j in peers:
            pltpu.make_async_remote_copy(
                src_ref=mem_buf.at[pl.ds(pl.multiple_of(128 * s + 8 * j, 8), 8), :],
                dst_ref=m_recv.at[slot_rows(s, 8), :],
                send_sem=m_ssem.at[s],
                recv_sem=m_rsem.at[s],
                device_id=(j, tp),
                device_id_type=MESH_ID,
            ).start()

    finished(p_copies[3:])
    start(s_copies[2][2:])
    chunk_dot(0, 3)
    finished(s_copies[1][:2])
    start(s_copies[3])
    chunk_dot(1, 0)
    chunk_dot(1, 1)
    suffix(0)
    finished(s_copies[1][2:])
    chunk_dot(1, 2)
    chunk_dot(1, 3)

    for copy in halo_copies:
        copy.wait_recv()
    finished(s_copies[2])
    finished(s_copies[3])
    col_buf[:, 8:16] = jnp.where(sp == 0, 0.0, jnp.transpose(h_recv[0]))
    col_buf[:, 16:24] = jnp.where(sp == sp_n - 1, 0.0, jnp.transpose(h_recv[1]))
    chunk_dot(2, 0)
    chunk_dot(2, 1)
    suffix(1)
    keys(0)
    weigh(0)

    own_ow = pltpu.make_async_copy(ow_cols(sp), ow_slot(ow_recv), ow_local)
    own_ow.start()
    f_recv[pl.ds(my_tile, 8), :] = f_buf[...]
    for j in peers:
        pltpu.make_async_remote_copy(
            src_ref=f_buf,
            dst_ref=f_recv.at[pl.ds(my_tile, 8), :],
            send_sem=f_ssem,
            recv_sem=f_rsem,
            device_id=(j, tp),
            device_id_type=MESH_ID,
        ).start()
        pltpu.make_async_remote_copy(
            src_ref=ow_cols(j),
            dst_ref=ow_slot(ow_recv),
            send_sem=ow_ssem,
            recv_sem=ow_rsem,
            device_id=(j, tp),
            device_id_type=MESH_ID,
        ).start()

    chunk_dot(2, 2)
    outer(0)
    chunk_dot(2, 3)
    chunk_dot(3, 0)
    keys(1)
    weigh(1)
    send_sums(0)
    send_memory(0)
    suffix(2)
    chunk_dot(3, 1)
    outer(1)
    chunk_dot(3, 2)
    send_sums(1)
    send_memory(1)
    keys(2)
    weigh(2)
    chunk_dot(3, 3)
    outer(2)
    suffix(3)
    send_sums(2)
    keys(3)
    weigh(3)
    outer(3)
    send_sums(3)
    send_memory(2)
    send_memory(3)

    def take(ref, sem, count):
        view = ref.at[pl.ds(0, count), :]
        pltpu.make_async_copy(view, view, sem).wait()

    own_ow.wait()
    ow_bytes = out_w.at[:, :, pl.ds(0, cols_of * (sp_n - 1))]
    pltpu.make_async_copy(ow_bytes, ow_bytes, ow_rsem).wait()
    ow_buf[...] = ow_recv[...].reshape(256, cols_of)
    take(f_recv, f_rsem, 8 * (sp_n - 1))
    fresh_sum = f_recv[0:8, :]
    for i in range(1, sp_n):
        fresh_sum = fresh_sum + f_recv[8 * i : 8 * i + 8, :]

    row16 = lax.broadcasted_iota(jnp.int32, (sp_n, 128), 0)
    low_lanes = lax.rem(lax.broadcasted_iota(jnp.int32, (sp_n, 128), 1), 64) < 32

    def by_head(x):
        left = jnp.sum(jnp.where(first_head, x, 0.0), axis=1, keepdims=True)
        right = jnp.sum(jnp.where(first_head, 0.0, x), axis=1, keepdims=True)
        return halves(left, right)

    def combine(s):
        def rows_at(k):
            return e_recv[pl.ds(s * sp_n * 4 + k, sp_n, stride=4), :]

        stats = rows_at(3)
        totals = jnp.where(low_lanes, stats, pltpu.roll(stats, 32, 1))
        tops = jnp.where(low_lanes, pltpu.roll(stats, 96, 1), stats)
        later = jnp.where(row16 < sp_n - 1, pltpu.roll(totals, sp_n - 1, 0), 0.0)
        shift = 1
        while shift < sp_n:
            later = later + jnp.where(
                row16 < sp_n - shift, pltpu.roll(later, sp_n - shift, 0), 0.0
            )
            shift *= 2
        gate = tops + later
        peak = jnp.max(gate, axis=0, keepdims=True)
        factor = jnp.exp(gate - peak)

        def summed(k):
            return jnp.sum(factor * rows_at(k), axis=0, keepdims=True)

        norm, num_a, num_b = summed(0), summed(1), summed(2)
        q, k = par_buf[0, s : s + 1, :], par_buf[1, s : s + 1, :]
        gate_in, gate_fg = par_buf[2, s : s + 1, :], par_buf[3, s : s + 1, :]
        kept = log_sigmoid(gate_fg) + peak
        new_peak = jnp.maximum(kept, gate_in)
        old_scale = jnp.exp(kept - new_peak)
        new_scale = jnp.exp(gate_in - new_peak)
        denom = jnp.maximum(jnp.abs(by_head(q * (old_scale * norm + new_scale * k))), 1.0)
        fresh_scale = new_scale * by_head(q * k)
        read_a = (old_scale * num_a + fresh_scale * fresh_sum[s : s + 1]) / denom
        read_b = (old_scale * num_b + fresh_scale * fresh_sum[4 + s : 5 + s]) / denom
        packed[32 + s : 33 + s, :] = pltpu.roll(norm, lax.rem(128 - 4 * sp, 128), 1)
        packed[36 + s : 37 + s, :] = peak
        return jnp.concatenate([read_a, read_b], axis=1), factor

    reads, factors = [], []
    for s in range(seqs - 1):
        take(e_recv, e_rsem.at[s], 4 * (sp_n - 1))
        row, factor = combine(s)
        reads.append(row)
        factors.append(factor)
    take(e_recv, e_rsem.at[seqs - 1], 4 * (sp_n - 1))
    row, factor = combine(seqs - 1)
    reads.append(row)
    factors.append(factor)

    read = jnp.concatenate(reads + [jnp.zeros((12, 256), F32)], axis=0).astype(BF16)
    part = jnp.dot(read, ow_buf[...], preferred_element_type=F32)[0:4]
    part_buf[0] = part[:, 0:128]
    part_buf[1] = part[:, 128:256]
    part_recv[tp] = part_buf[tp // 4]
    y, core = tp // 2, lax.rem(tp, 2)
    for dy, dc in ((2, 1), (2, 0), (1, 1), (3, 1), (1, 0), (3, 0), (0, 1)):
        j = lax.rem(y + dy, 4) * 2 + lax.rem(core + dc, 2)
        pltpu.make_async_remote_copy(
            src_ref=part_buf.at[j // 4],
            dst_ref=part_recv.at[tp],
            send_sem=o_ssem,
            recv_sem=o_rsem,
            device_id=(sp, j),
            device_id_type=MESH_ID,
        ).start()

    for s in range(seqs):
        take(m_recv, m_rsem.at[s], 8 * (sp_n - 1))
    for s in range(seqs):
        memory = jnp.zeros((8, 128), F32)
        for i in range(sp_n):
            base = (s * sp_n + i) * 8
            memory = memory + factors[s][i : i + 1] * m_recv[base : base + 8, :]
        packed[8 * s : 8 * s + 8, :] = memory

    view = part_recv.at[pl.ds(0, tp_n - 1)]
    pltpu.make_async_copy(view, view, o_rsem).wait()
    whole = part_recv[0]
    for i in range(1, tp_n):
        whole = whole + part_recv[i]
    packed[40:44, :] = pltpu.roll(whole, lax.rem(128 - 32 * lax.rem(tp, 4), 128), 1)

    for copy in halo_copies:
        copy.wait_send()
    pltpu.make_async_copy(ow_bytes, ow_bytes, ow_ssem).wait()
    take(f_recv, f_ssem, 8 * (sp_n - 1))
    for s in range(seqs):
        take(e_recv, e_ssem.at[s], 4 * (sp_n - 1))
        take(m_recv, m_ssem.at[s], 8 * (sp_n - 1))
    pltpu.make_async_copy(view, view, o_ssem).wait()


def unpack(packed, mem_out, norm_out, peak_out, read_out):
    seqs = mem_out.shape[0]
    for s in range(seqs):
        rows = packed[8 * s : 8 * s + 8, :]
        mem_out[s, 0] = rows[:, 0:64].astype(BF16)
        mem_out[s, 1] = rows[:, 64:128].astype(BF16)
        norm = packed[32 + s : 33 + s, :]
        norm_out[s, 0:1, :] = norm[:, 0:4].astype(BF16)
        norm_out[s, 1:2, :] = norm[:, 64:68].astype(BF16)
        peak = packed[36 + s : 37 + s, :]
        peak_out[0:1, s : s + 1] = peak[:, 0:1]
        peak_out[1:2, s : s + 1] = peak[:, 64:65]
    read_out[...] = packed[40:44, 0:32].astype(BF16)


def body(
    prompt, key_weight, value_weight, input_gate_weight, forget_gate_weight, forget_bias,
    key_taps, extra_decay, new_query, new_key, new_value, new_input_gate, new_forget_gate,
    out_weight,
):
    seqs, length, width = prompt.shape
    sp_n = lax.axis_size("sp")
    tp_n = lax.axis_size("tp")
    cols_of = out_weight.shape[2] // sp_n
    any_spec = pl.BlockSpec(memory_space=pl.ANY)
    vmem = pl.BlockSpec(memory_space=pltpu.VMEM)
    dma = pltpu.SemaphoreType.DMA
    packed = pl.pallas_call(
        kernel,
        out_shape=pltpu.VMEM((48, 128), F32),
        in_specs=[any_spec] * 14,
        out_specs=vmem,
        scratch_shapes=[
            pltpu.VMEM((seqs, length, width), BF16),
            pltpu.VMEM((width, 128), BF16),
            pltpu.VMEM((width, 256), BF16),
            pltpu.VMEM((400, width), BF16),
            pltpu.VMEM((64, width), BF16),
            pltpu.VMEM((seqs, 400, length), F32),
            pltpu.VMEM((length, length), BF16),
            pltpu.VMEM((4, 8, 128), F32),
            pltpu.VMEM((seqs * 128, 128), F32),
            pltpu.VMEM((seqs * 4, 128), F32),
            pltpu.VMEM((2, 8, 128), F32),
            pltpu.VMEM((2, 8, 128), F32),
            pltpu.VMEM((seqs * sp_n * 4, 128), F32),
            pltpu.VMEM((seqs * sp_n * 8, 128), F32),
            pltpu.VMEM((2, 2, 8, 8, cols_of), BF16),
            pltpu.VMEM((2, 4, 128), F32),
            pltpu.VMEM((tp_n, 4, 128), F32),
            pltpu.VMEM((8, 128), F32),
            pltpu.VMEM((sp_n * 8, 128), F32),
            pltpu.VMEM((seqs, 272, length), BF16),
            pltpu.VMEM((seqs, 128, length), BF16),
            pltpu.VMEM((seqs, 16, length), BF16),
            pltpu.VMEM((seqs, 4, length), F32),
            pltpu.VMEM((256, cols_of), BF16),
            pltpu.VMEM((128, 128), F32),
            pltpu.VMEM((2, width), BF16),
            pltpu.VMEM((2, width), BF16),
            pltpu.SMEM((2,), F32),
            pltpu.VMEM((3, 128), BF16),
            pltpu.VMEM((seqs, 2, length), F32),
            pltpu.VMEM((seqs, 2, 64), BF16),
            pltpu.VMEM((seqs, 2, 64), BF16),
            pltpu.VMEM((seqs, 2, 8), BF16),
            pltpu.VMEM((2, seqs), F32),
            pltpu.VMEM((2, seqs), F32),
            dma((2, CHUNKS)),
            dma((seqs, CHUNKS)),
            dma((2 * seqs,)),
            dma((10,)),
            dma,
            dma((2,)),
            dma((2,)),
            dma((seqs,)),
            dma((seqs,)),
            dma((seqs,)),
            dma((seqs,)),
            dma,
            dma,
            dma,
            dma,
            dma,
            dma,
        ],
        compiler_params=pltpu.CompilerParams(
            collective_id=0, has_side_effects=True, vmem_limit_bytes=60 * 1024 * 1024
        ),
        name="prompt_state",
    )(
        prompt,
        key_weight,
        value_weight,
        input_gate_weight.T,
        forget_gate_weight.T,
        forget_bias,
        key_taps,
        jnp.transpose(extra_decay, (0, 2, 1)),
        new_query,
        new_key,
        new_value,
        new_input_gate.T,
        new_forget_gate.T,
        out_weight,
    )
    memory, norm, peak, read = pl.pallas_call(
        unpack,
        out_shape=(
            jax.ShapeDtypeStruct((seqs, 2, 8, 64), BF16),
            jax.ShapeDtypeStruct((seqs, 2, 4), BF16),
            jax.ShapeDtypeStruct((2, seqs), F32),
            jax.ShapeDtypeStruct((seqs, 32), BF16),
        ),
        in_specs=[vmem],
        out_specs=(vmem,) * 4,
        compiler_params=pltpu.CompilerParams(vmem_limit_bytes=1024 * 1024),
        name="unpack",
    )(packed)
    return jnp.transpose(memory, (0, 1, 3, 2)), norm, peak.T, read


def solution(mesh):
    in_specs = (
        P(None, "sp", None),
        P(None, "tp"),
        P(None, "tp"),
        P(None, "tp"),
        P(None, "tp"),
        P("tp"),
        P(None, "tp"),
        P(None, "sp", "tp"),
        P(None, "tp", None),
        P(None, "tp", None),
        P(None, "tp", "sp"),
        P(None, "tp"),
        P(None, "tp"),
        P("tp", "sp", None),
    )
    out_specs = (
        P(None, "tp", None, "sp"),
        P(None, "tp", "sp"),
        P(None, "tp"),
        P(None, ("sp", "tp")),
    )
    return jax.shard_map(body, mesh=mesh, in_specs=in_specs, out_specs=out_specs, check_vma=False)
```

time: 33.3 us -> 29.2 us (0.88)
  Pallas kernels: 32.5 us -> 28.4 us
    pallas_call x1, Pallas kernels: 31.8 us -> 27.7 us  [body(): pl.pallas_call(kernel, out_shape=pltpu.VMEM((48, 128), F32), in_specs=[an...]
where the time goes in v3:
time: 29.2 us; the launch traced here: 29.1 us
  Pallas kernels  28.4 us (97%)
  between operations  0.64 us (2%)
    pallas_call x1, Pallas kernels, body(): pl.pallas_call(kernel, out_shape=pltpu.VMEM((48, 128), F32), in_specs=[an...  27.7 us
    pallas_call x1, Pallas kernels, body(): pl.pallas_call(unpack, out_shape=(jax.ShapeDtypeStruct((seqs, 2, 8, 64),...  0.7 us

profile of v3, /device:TPU:1, one launch (start us, length us, event | category | flops | bytes accessed | tf_op | source)
XLA Modules:
  0.0 29.1 jit_solution(16145374225545873532)
XLA Ops:
  0.6 27.7 %prompt_state.1.packed = f32[48,128]{1,0:T(8,128)S(1)} custom-call(bf16[4,512,4096]{2,1,0:T(8,128)(2,1)} %prompt.1, bf16[4096,128]{1,0:T(8,128)(2,1)} %key_w.1, bf16[4096,256]{1,0:T(8,128)(2,1)} %value_w.1, bf16[2,4096]{1,0:T(2,128)(2,1)} %bitcast.7, bf16[2,4096]{1,0:T(2,128)(2,1)} %bitcast.8, f32[2]{0:T(128)} %fg_bias.1, bf16[3,128]{1,0:T(4,128)(2,1)} %taps.1, ...), custom_call_target="tpu_custom_call" | custom-call | tf_op jit(solution)/shard_map/prompt_state/pallas_call | solution.py:549
  28.4 0.7 %unpack.1 = (bf16[4,2,8,64]{3,2,1,0:T(8,128)(2,1)}, bf16[4,2,4]{2,1,0:T(2,128)(2,1)}, f32[2,4]{1,0:T(2,128)}, bf16[4,32]{1,0:T(4,128)(2,1)}) custom-call(f32[48,128]{1,0:T(8,128)S(1)} %prompt_state.1.packed), custom_call_target="tpu_custom_call" | custom-call | tf_op jit(solution)/shard_map/unpack/pallas_call | solution.py:628

commit v4 on v3

--- a/solution.py
+++ b/solution.py
@@ -106,6 +106,8 @@
     start(small_copies)
     start(w_copies[1:2])
     start(p_copies[1:2])
+    start(w_copies[2:3])
+    start(p_copies[2:3])
 
     @pl.loop(1, sp_n)
     def _(d):
@@ -131,6 +133,7 @@
 
     def turn(c):
         cols = chunk_of(c)
+        wt_buf[KEY0:VAL0, cols] = jnp.transpose(wk_buf[cols, :])
         wt_buf[VAL0:, cols] = jnp.transpose(wv_buf[cols, :])
 
     def chunk_dot(s, c):
@@ -144,13 +147,12 @@
             r_buf[s] = r_buf[s] + part
 
     finished(wk_copies)
-    start(w_copies[2:])
-    start(p_copies[2:])
-    for c in range(CHUNKS):
-        cols = chunk_of(c)
-        wt_buf[KEY0:VAL0, cols] = jnp.transpose(wk_buf[cols, :])
     finished(hp_copies)
-
+    finished(small_copies)
+    finished(w_copies[:1])
+    start(w_copies[3:])
+    start(p_copies[3:])
+    start(s_copies[1][:2])
     edge = jnp.dot(hp_buf[...], wk_buf[...], preferred_element_type=F32).astype(BF16).astype(F32)
     zero4 = jnp.zeros((4, 128), F32)
     h_send[0] = jnp.concatenate(
@@ -160,7 +162,6 @@
         [edge[16 * s : 16 * s + 1] for s in range(seqs)] + [zero4], axis=0
     )
 
-    finished(small_copies)
     gate_rows = jnp.concatenate(
         [
             in_v[...].astype(F32), jnp.zeros((6, width), F32),
@@ -169,9 +170,8 @@
         axis=0,
     )
     wt_buf[0:KEY0, :] = gate_rows.astype(BF16)
-    finished(w_copies[:1])
-    start(s_copies[1][:2])
     turn(0)
+
     finished(p_copies[:1])
     finished(w_copies[1:2])
     start(s_copies[1][2:])
@@ -191,15 +191,13 @@
         copy.start()
         halo_copies.append(copy)
 
-    finished(p_copies[1:2])
-    finished(w_copies[2:3])
+    finished(p_copies[1:3])
+    finished(w_copies[2:])
+    start(s_copies[2])
+    turn(2)
     chunk_dot(0, 1)
-    turn(2)
-    finished(p_copies[2:3])
-    finished(w_copies[3:])
-    start(s_copies[2][:2])
+    turn(3)
     chunk_dot(0, 2)
-    turn(3)
 
     for s in range(seqs):
         rows = pl.ds(s, 1)
@@ -252,8 +250,17 @@
     def suffix(s):
         fg_pre = r_buf[s, 8:10, :].astype(BF16).astype(F32)
         log_f = log_sigmoid(fg_pre + bias_col) + extra_v[s]
-        sums = jnp.dot(rows_of(log_f), tri_buf[...], preferred_element_type=F32)
-        later = sums[0:2] + sums[2:4] + sums[4:6]
+        if s == seqs - 1:
+            sums = jnp.dot(rows_of(log_f), tri_buf[...], preferred_element_type=F32)
+            later = sums[0:2] + sums[2:4] + sums[4:6]
+        else:
+            later = jnp.where(pos < length - 1, pltpu.roll(log_f, length - 1, 1), 0.0)
+            shift = 1
+            while shift < length:
+                later = later + jnp.where(
+                    pos < length - shift, pltpu.roll(later, length - shift, 1), 0.0
+                )
+                shift *= 2
         suf_buf[s, 0:2, :] = later
         suf_buf[s, 2:4, :] = jnp.broadcast_to(later[:, 0:1] + log_f[:, 0:1], (2, length))
 
@@ -337,10 +344,9 @@
             ).start()
 
     finished(p_copies[3:])
-    start(s_copies[2][2:])
-    chunk_dot(0, 3)
     finished(s_copies[1][:2])
     start(s_copies[3])
+    chunk_dot(0, 3)
     chunk_dot(1, 0)
     chunk_dot(1, 1)
     suffix(0)
@@ -351,15 +357,9 @@
     for copy in halo_copies:
         copy.wait_recv()
     finished(s_copies[2])
-    finished(s_copies[3])
     col_buf[:, 8:16] = jnp.where(sp == 0, 0.0, jnp.transpose(h_recv[0]))
     col_buf[:, 16:24] = jnp.where(sp == sp_n - 1, 0.0, jnp.transpose(h_recv[1]))
     chunk_dot(2, 0)
-    chunk_dot(2, 1)
-    suffix(1)
-    keys(0)
-    weigh(0)
-
     own_ow = pltpu.make_async_copy(ow_cols(sp), ow_slot(ow_recv), ow_local)
     own_ow.start()
     f_recv[pl.ds(my_tile, 8), :] = f_buf[...]
@@ -381,22 +381,27 @@
             device_id_type=MESH_ID,
         ).start()
 
+    chunk_dot(2, 1)
+    keys(0)
+    weigh(0)
     chunk_dot(2, 2)
+    suffix(1)
+    chunk_dot(2, 3)
+
+    finished(s_copies[3])
     outer(0)
-    chunk_dot(2, 3)
     chunk_dot(3, 0)
     keys(1)
     weigh(1)
     send_sums(0)
     send_memory(0)
+    chunk_dot(3, 1)
     suffix(2)
-    chunk_dot(3, 1)
     outer(1)
     chunk_dot(3, 2)
-    send_sums(1)
-    send_memory(1)
     keys(2)
     weigh(2)
+    send_sums(1)
     chunk_dot(3, 3)
     outer(2)
     suffix(3)
@@ -405,6 +410,7 @@
     weigh(3)
     outer(3)
     send_sums(3)
+    send_memory(1)
     send_memory(2)
     send_memory(3)
 

time: 29.2 us -> 28.7 us (0.983)
  Pallas kernels: 28.4 us -> 27.9 us
    pallas_call x1, Pallas kernels: 27.7 us -> 27.2 us  [body(): pl.pallas_call(kernel, out_shape=pltpu.VMEM((48, 128), F32), in_specs=[an...]
where the time goes in v4:
time: 28.7 us; the launch traced here: 28.6 us
  Pallas kernels  27.9 us (97%)
  between operations  0.64 us (2%)
    pallas_call x1, Pallas kernels, body(): pl.pallas_call(kernel, out_shape=pltpu.VMEM((48, 128), F32), in_specs=[an...  27.2 us
    pallas_call x1, Pallas kernels, body(): pl.pallas_call(unpack, out_shape=(jax.ShapeDtypeStruct((seqs, 2, 8, 64),...  0.7 us

profile of v4, /device:TPU:1, one launch (start us, length us, event | category | flops | bytes accessed | tf_op | source)
XLA Modules:
  0.0 28.6 jit_solution(9876551953297397355)
XLA Ops:
  0.6 27.2 %prompt_state.1.packed = f32[48,128]{1,0:T(8,128)S(1)} custom-call(bf16[4,512,4096]{2,1,0:T(8,128)(2,1)} %prompt.1, bf16[4096,128]{1,0:T(8,128)(2,1)} %key_w.1, bf16[4096,256]{1,0:T(8,128)(2,1)} %value_w.1, bf16[2,4096]{1,0:T(2,128)(2,1)} %bitcast.7, bf16[2,4096]{1,0:T(2,128)(2,1)} %bitcast.8, f32[2]{0:T(128)} %fg_bias.1, bf16[3,128]{1,0:T(4,128)(2,1)} %taps.1, ...), custom_call_target="tpu_custom_call" | custom-call | tf_op jit(solution)/shard_map/prompt_state/pallas_call | solution.py:555
  27.9 0.7 %unpack.1 = (bf16[4,2,8,64]{3,2,1,0:T(8,128)(2,1)}, bf16[4,2,4]{2,1,0:T(2,128)(2,1)}, f32[2,4]{1,0:T(2,128)}, bf16[4,32]{1,0:T(4,128)(2,1)}) custom-call(f32[48,128]{1,0:T(8,128)S(1)} %prompt_state.1.packed), custom_call_target="tpu_custom_call" | custom-call | tf_op jit(solution)/shard_map/unpack/pallas_call | solution.py:634

commit v5 on v4

--- a/solution.py
+++ b/solution.py
@@ -65,29 +65,30 @@
             g = 2 * s + side
             hp_copies.append(
                 pltpu.make_async_copy(
-                    prompt.at[s, pl.ds(row, 8), :], hp_buf.at[pl.ds(8 * g, 8), :], hp_sem.at[g]
+                    prompt.at[s, pl.ds(row, 8), :], hp_buf.at[pl.ds(8 * g, 8), :], hp_sem
                 )
             )
     wk_copies = [
-        pltpu.make_async_copy(key_w.at[rows, :], wk_buf.at[rows, :], w_sem.at[0, i])
-        for i, rows in enumerate((pl.ds(0, width // 2), pl.ds(width // 2, width // 2)))
+        pltpu.make_async_copy(key_w.at[rows, :], wk_buf.at[rows, :], w_sem.at[0])
+        for rows in (pl.ds(0, width // 2), pl.ds(width // 2, width // 2))
     ]
     w_copies, p_copies = [], []
     for c in range(CHUNKS):
         rows = pl.ds(c * step, step)
         w_copies.append(
-            pltpu.make_async_copy(value_w.at[rows, :], wv_buf.at[rows, :], w_sem.at[1, c])
+            pltpu.make_async_copy(value_w.at[rows, :], wv_buf.at[rows, :], w_sem.at[1 + c])
         )
         p_copies.append(
-            pltpu.make_async_copy(prompt.at[0, :, rows], p_buf.at[0, :, rows], p_sem.at[0, c])
+            pltpu.make_async_copy(prompt.at[0, :, rows], p_buf.at[0, :, rows], p_sem.at[c])
         )
     s_copies = [p_copies]
     for s in range(1, seqs):
         group = []
         for c in range(CHUNKS):
             cols = pl.ds(c * step, step)
+            s_sem = p_sem.at[CHUNKS + c // 2 if s == 1 else CHUNKS + s]
             group.append(
-                pltpu.make_async_copy(prompt.at[s, :, cols], p_buf.at[s, :, cols], p_sem.at[s, c])
+                pltpu.make_async_copy(prompt.at[s, :, cols], p_buf.at[s, :, cols], s_sem)
             )
         s_copies.append(group)
 
@@ -98,6 +99,9 @@
     def finished(copies):
         for copy in copies:
             copy.wait()
+
+    def landed(view, sem):
+        pltpu.make_async_copy(view, view, sem).wait()
 
     start(wk_copies)
     start(hp_copies)
@@ -146,8 +150,8 @@
         else:
             r_buf[s] = r_buf[s] + part
 
-    finished(wk_copies)
-    finished(hp_copies)
+    landed(wk_buf, w_sem.at[0])
+    landed(hp_buf, hp_sem)
     finished(small_copies)
     finished(w_copies[:1])
     start(w_copies[3:])
@@ -178,26 +182,26 @@
     chunk_dot(0, 0)
     turn(1)
     pl.semaphore_wait(barrier, sp_n - 1 + tp_n - 1)
-    halo_copies = []
     for side, d in ((0, 1), (1, sp_n - 1)):
         copy = pltpu.make_async_remote_copy(
             src_ref=h_send.at[side],
             dst_ref=h_recv.at[side],
-            send_sem=h_ssem.at[side],
-            recv_sem=h_rsem.at[side],
+            send_sem=h_ssem,
+            recv_sem=h_rsem,
             device_id=(sp_peer(d), tp),
             device_id_type=MESH_ID,
         )
         copy.start()
-        halo_copies.append(copy)
-
-    finished(p_copies[1:3])
-    finished(w_copies[2:])
+
+    finished(p_copies[1:2])
+    finished(w_copies[2:3])
+    chunk_dot(0, 1)
+    turn(2)
+    finished(p_copies[2:3])
+    finished(w_copies[3:])
     start(s_copies[2])
-    turn(2)
-    chunk_dot(0, 1)
+    chunk_dot(0, 2)
     turn(3)
-    chunk_dot(0, 2)
 
     for s in range(seqs):
         rows = pl.ds(s, 1)
@@ -325,8 +329,8 @@
             pltpu.make_async_remote_copy(
                 src_ref=e_buf.at[pl.ds(4 * s, 4), :],
                 dst_ref=e_recv.at[slot_rows(s, 4), :],
-                send_sem=e_ssem.at[s],
-                recv_sem=e_rsem.at[s],
+                send_sem=e_ssem,
+                recv_sem=e_rsem.at[s // (seqs - 1)],
                 device_id=(j, tp),
                 device_id_type=MESH_ID,
             ).start()
@@ -337,26 +341,25 @@
             pltpu.make_async_remote_copy(
                 src_ref=mem_buf.at[pl.ds(pl.multiple_of(128 * s + 8 * j, 8), 8), :],
                 dst_ref=m_recv.at[slot_rows(s, 8), :],
-                send_sem=m_ssem.at[s],
-                recv_sem=m_rsem.at[s],
+                send_sem=m_ssem,
+                recv_sem=m_rsem,
                 device_id=(j, tp),
                 device_id_type=MESH_ID,
             ).start()
 
     finished(p_copies[3:])
-    finished(s_copies[1][:2])
+    landed(p_buf.at[1, :, pl.ds(0, width // 2)], p_sem.at[CHUNKS])
     start(s_copies[3])
     chunk_dot(0, 3)
     chunk_dot(1, 0)
     chunk_dot(1, 1)
     suffix(0)
-    finished(s_copies[1][2:])
+    landed(p_buf.at[1, :, pl.ds(width // 2, width // 2)], p_sem.at[CHUNKS + 1])
     chunk_dot(1, 2)
     chunk_dot(1, 3)
 
-    for copy in halo_copies:
-        copy.wait_recv()
-    finished(s_copies[2])
+    landed(h_recv, h_rsem)
+    landed(p_buf.at[2], p_sem.at[CHUNKS + 2])
     col_buf[:, 8:16] = jnp.where(sp == 0, 0.0, jnp.transpose(h_recv[0]))
     col_buf[:, 16:24] = jnp.where(sp == sp_n - 1, 0.0, jnp.transpose(h_recv[1]))
     chunk_dot(2, 0)
@@ -388,7 +391,7 @@
     suffix(1)
     chunk_dot(2, 3)
 
-    finished(s_copies[3])
+    landed(p_buf.at[3], p_sem.at[CHUNKS + 3])
     outer(0)
     chunk_dot(3, 0)
     keys(1)
@@ -472,12 +475,12 @@
         return jnp.concatenate([read_a, read_b], axis=1), factor
 
     reads, factors = [], []
+    take(e_recv, e_rsem.at[0], 4 * (sp_n - 1) * (seqs - 1))
     for s in range(seqs - 1):
-        take(e_recv, e_rsem.at[s], 4 * (sp_n - 1))
         row, factor = combine(s)
         reads.append(row)
         factors.append(factor)
-    take(e_recv, e_rsem.at[seqs - 1], 4 * (sp_n - 1))
+    take(e_recv, e_rsem.at[1], 4 * (sp_n - 1))
     row, factor = combine(seqs - 1)
     reads.append(row)
     factors.append(factor)
@@ -499,8 +502,7 @@
             device_id_type=MESH_ID,
         ).start()
 
-    for s in range(seqs):
-        take(m_recv, m_rsem.at[s], 8 * (sp_n - 1))
+    take(m_recv, m_rsem, 8 * (sp_n - 1) * seqs)
     for s in range(seqs):
         memory = jnp.zeros((8, 128), F32)
         for i in range(sp_n):
@@ -515,13 +517,11 @@
         whole = whole + part_recv[i]
     packed[40:44, :] = pltpu.roll(whole, lax.rem(128 - 32 * lax.rem(tp, 4), 128), 1)
 
-    for copy in halo_copies:
-        copy.wait_send()
+    landed(h_recv, h_ssem)
     pltpu.make_async_copy(ow_bytes, ow_bytes, ow_ssem).wait()
     take(f_recv, f_ssem, 8 * (sp_n - 1))
-    for s in range(seqs):
-        take(e_recv, e_ssem.at[s], 4 * (sp_n - 1))
-        take(m_recv, m_ssem.at[s], 8 * (sp_n - 1))
+    take(e_recv, e_ssem, 4 * (sp_n - 1) * seqs)
+    take(m_recv, m_ssem, 8 * (sp_n - 1) * seqs)
     pltpu.make_async_copy(view, view, o_ssem).wait()
 
 
@@ -593,17 +593,17 @@
             pltpu.VMEM((seqs, 2, 8), BF16),
             pltpu.VMEM((2, seqs), F32),
             pltpu.VMEM((2, seqs), F32),
-            dma((2, CHUNKS)),
-            dma((seqs, CHUNKS)),
-            dma((2 * seqs,)),
+            dma((1 + CHUNKS,)),
+            dma((CHUNKS + seqs,)),
+            dma,
             dma((10,)),
             dma,
+            dma,
+            dma,
+            dma,
             dma((2,)),
-            dma((2,)),
-            dma((seqs,)),
-            dma((seqs,)),
-            dma((seqs,)),
-            dma((seqs,)),
+            dma,
+            dma,
             dma,
             dma,
             dma,

time: 28.7 us -> 28.4 us (0.990)
  Pallas kernels: 27.9 us -> 27.6 us
    pallas_call x1, Pallas kernels: 27.2 us -> 26.9 us  [body(): pl.pallas_call(kernel, out_shape=pltpu.VMEM((48, 128), F32), in_specs=[an...]
where the time goes in v5:
time: 28.4 us; the launch traced here: 28.3 us
  Pallas kernels  27.6 us (97%)
  between operations  0.64 us (2%)
    pallas_call x1, Pallas kernels, body(): pl.pallas_call(kernel, out_shape=pltpu.VMEM((48, 128), F32), in_specs=[an...  26.9 us
    pallas_call x1, Pallas kernels, body(): pl.pallas_call(unpack, out_shape=(jax.ShapeDtypeStruct((seqs, 2, 8, 64),...  0.7 us

profile of v5, /device:TPU:1, one launch (start us, length us, event | category | flops | bytes accessed | tf_op | source)
XLA Modules:
  0.0 28.3 jit_solution(17871711949538964975)
XLA Ops:
  0.6 26.9 %prompt_state.1.packed = f32[48,128]{1,0:T(8,128)S(1)} custom-call(bf16[4,512,4096]{2,1,0:T(8,128)(2,1)} %prompt.1, bf16[4096,128]{1,0:T(8,128)(2,1)} %key_w.1, bf16[4096,256]{1,0:T(8,128)(2,1)} %value_w.1, bf16[2,4096]{1,0:T(2,128)(2,1)} %bitcast.7, bf16[2,4096]{1,0:T(2,128)(2,1)} %bitcast.8, f32[2]{0:T(128)} %fg_bias.1, bf16[3,128]{1,0:T(4,128)(2,1)} %taps.1, ...), custom_call_target="tpu_custom_call" | custom-call | tf_op jit(solution)/shard_map/prompt_state/pallas_call | solution.py:555
  27.6 0.7 %unpack.1 = (bf16[4,2,8,64]{3,2,1,0:T(8,128)(2,1)}, bf16[4,2,4]{2,1,0:T(2,128)(2,1)}, f32[2,4]{1,0:T(2,128)}, bf16[4,32]{1,0:T(4,128)(2,1)}) custom-call(f32[48,128]{1,0:T(8,128)S(1)} %prompt_state.1.packed), custom_call_target="tpu_custom_call" | custom-call | tf_op jit(solution)/shard_map/unpack/pallas_call | solution.py:634

commit v6 on v5

--- a/solution.py
+++ b/solution.py
@@ -92,9 +92,9 @@
             )
         s_copies.append(group)
 
-    def start(copies):
+    def start(copies, priority=0):
         for copy in copies:
-            copy.start()
+            copy.start(priority=priority)
 
     def finished(copies):
         for copy in copies:
@@ -108,10 +108,10 @@
     start(w_copies[:1])
     start(p_copies[:1])
     start(small_copies)
-    start(w_copies[1:2])
-    start(p_copies[1:2])
-    start(w_copies[2:3])
-    start(p_copies[2:3])
+    start(w_copies[1:2], 1)
+    start(p_copies[1:2], 1)
+    start(w_copies[2:3], 1)
+    start(p_copies[2:3], 1)
 
     @pl.loop(1, sp_n)
     def _(d):
@@ -154,9 +154,9 @@
     landed(hp_buf, hp_sem)
     finished(small_copies)
     finished(w_copies[:1])
-    start(w_copies[3:])
-    start(p_copies[3:])
-    start(s_copies[1][:2])
+    start(w_copies[3:], 1)
+    start(p_copies[3:], 1)
+    start(s_copies[1][:2], 1)
     edge = jnp.dot(hp_buf[...], wk_buf[...], preferred_element_type=F32).astype(BF16).astype(F32)
     zero4 = jnp.zeros((4, 128), F32)
     h_send[0] = jnp.concatenate(
@@ -178,7 +178,7 @@
 
     finished(p_copies[:1])
     finished(w_copies[1:2])
-    start(s_copies[1][2:])
+    start(s_copies[1][2:], 1)
     chunk_dot(0, 0)
     turn(1)
     pl.semaphore_wait(barrier, sp_n - 1 + tp_n - 1)
@@ -199,7 +199,7 @@
     turn(2)
     finished(p_copies[2:3])
     finished(w_copies[3:])
-    start(s_copies[2])
+    start(s_copies[2], 1)
     chunk_dot(0, 2)
     turn(3)
 
@@ -270,9 +270,19 @@
 
     def keys(s):
         key = r_buf[s, KEY0:VAL0, :].astype(BF16).astype(F32)
-        earlier = jnp.where(pos == 0, col_buf[:, 8 + s : 9 + s], pltpu.roll(key, 1, 1))
-        coming = jnp.where(
-            pos == length - 1, col_buf[:, 16 + s : 17 + s], pltpu.roll(key, length - 1, 1)
+        edge = length - 128
+        earlier = pltpu.roll(key, 1, 1)
+        earlier = jnp.concatenate(
+            [jnp.where(lane == 0, col_buf[:, 8 + s : 9 + s], earlier[:, :128]), earlier[:, 128:]],
+            axis=1,
+        )
+        coming = pltpu.roll(key, length - 1, 1)
+        coming = jnp.concatenate(
+            [
+                coming[:, :edge],
+                jnp.where(lane == 127, col_buf[:, 16 + s : 17 + s], coming[:, edge:]),
+            ],
+            axis=1,
         )
         mixed = col_buf[:, 0:1] * earlier + col_buf[:, 1:2] * key + col_buf[:, 2:3] * coming
         key_rows = (mixed * jax.nn.sigmoid(mixed) * 0.125).astype(BF16)
@@ -349,7 +359,7 @@
 
     finished(p_copies[3:])
     landed(p_buf.at[1, :, pl.ds(0, width // 2)], p_sem.at[CHUNKS])
-    start(s_copies[3])
+    start(s_copies[3], 1)
     chunk_dot(0, 3)
     chunk_dot(1, 0)
     chunk_dot(1, 1)

time: 28.4 us -> 28.4 us (level)
  no operation moved by 1% of the time
where the time goes in v6:
time: 28.4 us; the launch traced here: 28.3 us
  Pallas kernels  27.7 us (98%)
  between operations  0.64 us (2%)
    pallas_call x1, Pallas kernels, body(): pl.pallas_call(kernel, out_shape=pltpu.VMEM((48, 128), F32), in_specs=[an...  27 us
    pallas_call x1, Pallas kernels, body(): pl.pallas_call(unpack, out_shape=(jax.ShapeDtypeStruct((seqs, 2, 8, 64),...  0.7 us

profile of v6, /device:TPU:1, one launch (start us, length us, event | category | flops | bytes accessed | tf_op | source)
XLA Modules:
  0.0 28.3 jit_solution(14055243462258260551)
XLA Ops:
  0.6 27.0 %prompt_state.1.packed = f32[48,128]{1,0:T(8,128)S(1)} custom-call(bf16[4,512,4096]{2,1,0:T(8,128)(2,1)} %prompt.1, bf16[4096,128]{1,0:T(8,128)(2,1)} %key_w.1, bf16[4096,256]{1,0:T(8,128)(2,1)} %value_w.1, bf16[2,4096]{1,0:T(2,128)(2,1)} %bitcast.7, bf16[2,4096]{1,0:T(2,128)(2,1)} %bitcast.8, f32[2]{0:T(128)} %fg_bias.1, bf16[3,128]{1,0:T(4,128)(2,1)} %taps.1, ...), custom_call_target="tpu_custom_call" | custom-call | tf_op jit(solution)/shard_map/prompt_state/pallas_call | solution.py:565
  27.6 0.7 %unpack.1 = (bf16[4,2,8,64]{3,2,1,0:T(8,128)(2,1)}, bf16[4,2,4]{2,1,0:T(2,128)(2,1)}, f32[2,4]{1,0:T(2,128)}, bf16[4,32]{1,0:T(4,128)(2,1)}) custom-call(f32[48,128]{1,0:T(8,128)S(1)} %prompt_state.1.packed), custom_call_target="tpu_custom_call" | custom-call | tf_op jit(solution)/shard_map/unpack/pallas_call | solution.py:644

commit v7 on v6

--- a/solution.py
+++ b/solution.py
@@ -368,10 +368,7 @@
     chunk_dot(1, 2)
     chunk_dot(1, 3)
 
-    landed(h_recv, h_rsem)
     landed(p_buf.at[2], p_sem.at[CHUNKS + 2])
-    col_buf[:, 8:16] = jnp.where(sp == 0, 0.0, jnp.transpose(h_recv[0]))
-    col_buf[:, 16:24] = jnp.where(sp == sp_n - 1, 0.0, jnp.transpose(h_recv[1]))
     chunk_dot(2, 0)
     own_ow = pltpu.make_async_copy(ow_cols(sp), ow_slot(ow_recv), ow_local)
     own_ow.start()
@@ -395,10 +392,13 @@
         ).start()
 
     chunk_dot(2, 1)
+    suffix(1)
+    landed(h_recv, h_rsem)
+    col_buf[:, 8:16] = jnp.where(sp == 0, 0.0, jnp.transpose(h_recv[0]))
+    col_buf[:, 16:24] = jnp.where(sp == sp_n - 1, 0.0, jnp.transpose(h_recv[1]))
     keys(0)
     weigh(0)
     chunk_dot(2, 2)
-    suffix(1)
     chunk_dot(2, 3)
 
     landed(p_buf.at[3], p_sem.at[CHUNKS + 3])

time: 28.4 us -> 28.1 us (0.989)
  Pallas kernels: 27.7 us -> 27.3 us
    pallas_call x1, Pallas kernels: 27 us -> 26.6 us  [body(): pl.pallas_call(kernel, out_shape=pltpu.VMEM((48, 128), F32), in_specs=[an...]
where the time goes in v7:
time: 28.1 us; the launch traced here: 27.9 us
  Pallas kernels  27.3 us (97%)
  between operations  0.64 us (2%)
    pallas_call x1, Pallas kernels, body(): pl.pallas_call(kernel, out_shape=pltpu.VMEM((48, 128), F32), in_specs=[an...  26.6 us
    pallas_call x1, Pallas kernels, body(): pl.pallas_call(unpack, out_shape=(jax.ShapeDtypeStruct((seqs, 2, 8, 64),...  0.7 us

profile of v7, /device:TPU:1, one launch (start us, length us, event | category | flops | bytes accessed | tf_op | source)
XLA Modules:
  0.0 27.9 jit_solution(6148906224937603232)
XLA Ops:
  0.6 26.6 %prompt_state.1.packed = f32[48,128]{1,0:T(8,128)S(1)} custom-call(bf16[4,512,4096]{2,1,0:T(8,128)(2,1)} %prompt.1, bf16[4096,128]{1,0:T(8,128)(2,1)} %key_w.1, bf16[4096,256]{1,0:T(8,128)(2,1)} %value_w.1, bf16[2,4096]{1,0:T(2,128)(2,1)} %bitcast.7, bf16[2,4096]{1,0:T(2,128)(2,1)} %bitcast.8, f32[2]{0:T(128)} %fg_bias.1, bf16[3,128]{1,0:T(4,128)(2,1)} %taps.1, ...), custom_call_target="tpu_custom_call" | custom-call | tf_op jit(solution)/shard_map/prompt_state/pallas_call | solution.py:565
  27.2 0.7 %unpack.1 = (bf16[4,2,8,64]{3,2,1,0:T(8,128)(2,1)}, bf16[4,2,4]{2,1,0:T(2,128)(2,1)}, f32[2,4]{1,0:T(2,128)}, bf16[4,32]{1,0:T(4,128)(2,1)}) custom-call(f32[48,128]{1,0:T(8,128)S(1)} %prompt_state.1.packed), custom_call_target="tpu_custom_call" | custom-call | tf_op jit(solution)/shard_map/unpack/pallas_call | solution.py:644
